TPU v7x, 256 devices: a whole 4x4x8 slice. The times are simulated.
256 devices in a mesh: sp: 64 (over z, y, core), tp: 4 (over x).
Axes of the slice: x: 4, y: 4, z: 8, core: 2. Of those that a mesh axis runs over, the one named last changes fastest.
Arguments:
- queries: bfloat16 [32768, 1024], P('sp', 'tp'), may hold values from -6 to 6
- keys: bfloat16 [32768, 1024], P('sp', 'tp'), may hold values from -6 to 6
- values: bfloat16 [32768, 1024], P('sp', 'tp'), may hold values from -6 to 6
- output_gate_logits: bfloat16 [32768, 1024], P('sp', 'tp'), may hold values from -6 to 6
- input_gate_log: float32 [32768, 8], P('sp', 'tp'), may hold values from -5 to 125
- forget_gate_logits: float32 [32768, 8], P('sp', 'tp')
- extra_decay_log: float32 [32768, 8], P('sp', 'tp'), may hold values from -1 to 0
- document: int32 [32768], P('sp'), may hold values from 0 to 31, never falling along the last dimension, each value on 1 to 2048 neighbouring positions
- residual: bfloat16 [32768, 2048], P('sp', 'tp'), may hold values from -16 to 16
- cell_norm_gain: bfloat16 [1024], P('tp'), may hold values from 0.099609375 to 1.8984375
- output_weight: bfloat16 [1024, 2048], P('tp'), may hold values from -0.1875 to 0.1875
- mixer_norm_gain: bfloat16 [2048], P('tp'), may hold values from 0.099609375 to 1.8984375
- up_weight: bfloat16 [2048, 8192], P('sp', 'tp'), may hold values from -0.125 to 0.125
- down_weight: bfloat16 [8192, 2048], P('tp', 'sp'), may hold values from -0.0625 to 0.0625
Outputs:
- layer_out: bfloat16 [32768, 2048], P('sp', 'tp')
All inputs are finite; a program needn't handle non-finite values.
Results may differ from a plain program's by a relative error of at most 0.015.
Values may be sent and summed in bfloat16 or wider, within the bound.
No kernel may reach another device: no remote copies, remote signals or barrier semaphores. Data moves between devices by JAX's collectives and lax.ppermute only.
A program may use at most 128 MiB of HBM per device.

v0:
```python
import jax
import jax.numpy as jnp
from jax import lax
from jax.experimental import pallas as pl
from jax.experimental.pallas import tpu as pltpu
from jax.sharding import Mesh
from jax.sharding import PartitionSpec as P

NEG = -1e30
EPS = 1e-06
DH = 128
BLK = 128
NB = 4
HD = 2
TOK = 512
D = 2048
FF = 2048
SCALE = DH ** (-0.5)
BF = jnp.bfloat16
F32 = jnp.float32
HIGH = lax.Precision.HIGHEST
SP = ("z", "y", "c")
REL = (0, -1, 1, 2)


def shift(value, axis, by):
    count = lax.axis_size(axis)
    return lax.ppermute(value, axis, [(i, (i + by) % count) for i in range(count)])


def shift_sp(value, by):
    return lax.ppermute(value, SP, [(i, i + by) for i in range(64 - by)])


def split3(value):
    hi = value.astype(BF)
    rest = value - hi.astype(F32)
    mid = rest.astype(BF)
    low = (rest - mid.astype(F32)).astype(BF)
    return hi, mid, low


def block_sums(gates):
    tri = (
        lax.broadcasted_iota(jnp.int32, (BLK, BLK), 0)
        <= lax.broadcasted_iota(jnp.int32, (BLK, BLK), 1)
    ).astype(F32)
    cum = jnp.dot(gates[8:16, :], tri, precision=HIGH, preferred_element_type=F32)
    totals = [cum[r : r + 1, BLK - 1 : BLK] for r in range(8)]
    return cum, totals


def summary_part(gates_ref, k_ref, v_ref, out_ref):
    gates = gates_ref[...]
    cum, totals = block_sums(gates)
    docs = gates[16:24, :]
    last_doc = docs[3:4, BLK - 1 : BLK]
    rows, stabs, sums = [], [], []
    for h in range(HD):
        keeps = []
        after = jnp.zeros((1, 1), F32)
        for b in reversed(range(NB)):
            r = h * NB + b
            keep = (totals[r] - cum[r : r + 1, :]) + after + gates[r : r + 1, :]
            keeps.append(jnp.where(docs[b : b + 1, :] == last_doc, keep, NEG))
            after = after + totals[r]
        keeps = keeps[::-1]
        stab = jnp.max(keeps[0], axis=1, keepdims=True)
        for keep in keeps[1:]:
            stab = jnp.maximum(stab, jnp.max(keep, axis=1, keepdims=True))
        rows += [jnp.exp(keep - stab) for keep in keeps]
        stabs.append(stab)
        sums.append(after)
    columns = jnp.transpose(jnp.concatenate(rows, axis=0))
    norms = []
    for h in range(HD):
        scaled = jnp.concatenate(
            [
                k_ref[b * BLK : (b + 1) * BLK, h * DH : (h + 1) * DH].astype(F32)
                * columns[:, h * NB + b : h * NB + b + 1]
                for b in range(NB)
            ],
            axis=0,
        )
        norms.append(jnp.sum(scaled, axis=0, keepdims=True))
        memory = lax.dot_general(
            scaled.astype(BF),
            v_ref[:, h * DH : (h + 1) * DH],
            (((0,), (0,)), ((), ())),
            preferred_element_type=F32,
        )
        out_ref[h * DH : (h + 1) * DH, :] = memory.astype(BF)
    wide = lambda a: jnp.broadcast_to(a, (1, BLK))
    small = jnp.concatenate(
        norms
        + [wide(a) for a in stabs]
        + [wide(a) for a in sums]
        + [wide(last_doc + 1.0), jnp.zeros((1, BLK), F32)],
        axis=0,
    )
    hi, mid, low = split3(small)
    pad = jnp.zeros((8, BLK), F32)
    out_ref[256:272, :] = jnp.concatenate([hi.astype(F32), mid.astype(F32)], axis=0).astype(BF)
    out_ref[272:288, :] = jnp.concatenate([low.astype(F32), pad], axis=0).astype(BF)


def cell_kernel(gates_ref, q_ref, k_ref, v_ref, state_ref, numer_ref, aux_ref):
    summary_part(gates_ref, k_ref, v_ref, state_ref)
    gates = gates_ref[...]
    cum, totals = block_sums(gates)
    docs = gates[16:24, :]
    cum_cols = jnp.transpose(cum)
    doc_cols = jnp.transpose(docs)
    for b in range(NB):
        width = (b + 1) * BLK
        row_at = lax.broadcasted_iota(jnp.int32, (BLK, width), 0) + b * BLK
        col_at = lax.broadcasted_iota(jnp.int32, (BLK, width), 1)
        doc_row = jnp.concatenate([docs[a : a + 1, :] for a in range(b + 1)], axis=1)
        mask = (doc_cols[:, b : b + 1] == doc_row) & (col_at <= row_at)
        peaks, denoms = [], []
        for h in range(HD):
            r = h * NB + b
            parts = [gates[r : r + 1, :] - cum[r : r + 1, :]]
            between = jnp.zeros((1, 1), F32)
            for a in reversed(range(b)):
                ra = h * NB + a
                parts.append((totals[ra] - cum[ra : ra + 1, :]) + between + gates[ra : ra + 1, :])
                between = between + totals[ra]
            source = jnp.concatenate(parts[::-1], axis=1)
            pair = jnp.where(mask, cum_cols[:, r : r + 1] + source, NEG)
            peak = jnp.max(pair, axis=1, keepdims=True)
            lanes = slice(h * DH, (h + 1) * DH)
            scores = lax.dot_general(
                q_ref[b * BLK : (b + 1) * BLK, lanes],
                k_ref[0:width, lanes],
                (((1,), (1,)), ((), ())),
                preferred_element_type=F32,
            )
            scores = scores * SCALE * jnp.exp(pair - peak)
            denoms.append(jnp.sum(scores, axis=1, keepdims=True))
            peaks.append(peak)
            numer_ref[b * BLK : (b + 1) * BLK, lanes] = jnp.dot(
                scores.astype(BF), v_ref[0:width, lanes], preferred_element_type=F32
            )
        lane = lax.broadcasted_iota(jnp.int32, (BLK, BLK), 1)
        aux = jnp.where(
            lane == 0,
            peaks[0],
            jnp.where(lane == 1, peaks[1], jnp.where(lane == 2, denoms[0], denoms[1])),
        )
        aux_ref[b * BLK : (b + 1) * BLK, :] = aux


def combine_kernel(
    gates_ref, q_ref, og_ref, gain_ref, mixer_gain, numer_ref, aux_ref, s1, s2, s3, s4, full_ref, far_ref
):
    gates = gates_ref[...]
    cum, totals = block_sums(gates)
    docs = gates[16:24, :]
    cum_cols = jnp.transpose(cum)
    doc_cols = jnp.transpose(docs)
    doc0 = docs[0:1, 0:1]
    smalls = []
    for s in (s1, s2, s3, s4):
        upper = s[256:272, :].astype(F32)
        lower = s[272:288, :].astype(F32)
        smalls.append(upper[0:8, :] + upper[8:16, :] + lower[0:8, :])
    states = []
    for h in range(HD):
        far = jnp.zeros((1, 1), F32)
        logs, valids = [], []
        for small in smalls:
            valid = small[6:7, 0:1] == doc0 + 1.0
            logs.append(jnp.where(valid, small[2 + h : 3 + h, 0:1] + far, NEG))
            valids.append(valid)
            far = far + small[4 + h : 5 + h, 0:1]
        stab = jnp.maximum(jnp.maximum(logs[0], logs[1]), jnp.maximum(logs[2], logs[3]))
        memory = jnp.zeros((DH, DH), F32)
        normer = jnp.zeros((1, DH), F32)
        for s, small, log, valid in zip((s1, s2, s3, s4), smalls, logs, valids):
            weight = jnp.where(valid, jnp.exp(log - stab), 0.0)
            memory = memory + weight * s[h * DH : (h + 1) * DH, :].astype(F32)
            normer = normer + weight * small[h : h + 1, :]
        states.append((memory.astype(BF), normer, stab))
    before = [jnp.zeros((1, 1), F32) for _ in range(HD)]
    lane = lax.broadcasted_iota(jnp.int32, (BLK, BLK), 1)
    for b in range(NB):
        live = doc_cols[:, b : b + 1] == doc0
        far = []
        for h in range(HD):
            r = h * NB + b
            stab = states[h][2]
            log = cum_cols[:, r : r + 1] + (before[h] + stab)
            far.append(jnp.where(live & (stab > 0.5 * NEG), log, NEG))
            before[h] = before[h] + totals[r]
        far_ref[b] = jnp.where(lane == 0, far[0], far[1])

    def step(b, table):
        rows = pl.ds(pl.multiple_of(b * BLK, BLK), BLK)
        aux = aux_ref[rows, :]
        logs = far_ref[b]
        squares = jnp.zeros((BLK, 1), F32)
        for h in range(HD):
            lanes = slice(h * DH, (h + 1) * DH)
            memory, normer, _ = states[h]
            carried = logs[:, h : h + 1]
            peak = aux[:, h : h + 1]
            merged = jnp.maximum(peak, carried)
            own_w = jnp.exp(peak - merged)
            far_w = jnp.exp(carried - merged) * SCALE
            q_blk = q_ref[rows, lanes]
            numer = own_w * numer_ref[rows, lanes] + far_w * jnp.dot(
                q_blk, memory, preferred_element_type=F32
            )
            denom = own_w * aux[:, 2 + h : 3 + h] + far_w * jnp.sum(
                q_blk.astype(F32) * normer, axis=1, keepdims=True
            )
            cell = numer / jnp.maximum(jnp.abs(denom), 1.0)
            squares = squares + jnp.sum(cell * cell, axis=1, keepdims=True)
            gate = jax.nn.sigmoid(og_ref[rows, lanes].astype(F32))
            full_ref[rows, lanes] = (gate * cell * gain_ref[0:1, lanes].astype(F32)).astype(BF)
        return jnp.where(lane == b, squares, table)

    table = lax.fori_loop(0, NB, step, jnp.zeros((BLK, BLK), F32))
    hi, mid, low = (a.astype(F32) for a in split3(jnp.transpose(table)[0:8, :]))
    full_ref[TOK : TOK + 16, 0:128] = jnp.concatenate([hi, low], axis=0).astype(BF)
    gain = jnp.concatenate([mixer_gain[...].astype(F32), jnp.zeros((4, BLK), F32)], axis=0)
    full_ref[TOK : TOK + 16, 128:256] = jnp.concatenate([mid, gain], axis=0).astype(BF)


def block_of(at_ref, rel):
    return lax.rem(at_ref[3] + rel + 4, 4)


def project_kernel(at_ref, *refs):
    cells, own_resid, own_w = refs[0:4], refs[4], refs[5]
    packs, other = refs[6:9], refs[9]
    normed_ref, own_ref, w_ref, g_ref, r_ref, gain_ref, w_sem, r_sem = refs[10:]
    core = at_ref[2]
    weights = [pltpu.make_async_copy(own_w, w_ref.at[pl.ds(0, 256)], w_sem)]
    rows = [pltpu.make_async_copy(own_resid, r_ref.at[block_of(at_ref, 0)], r_sem)]
    for k, pack in enumerate(packs):
        parts = ((pack, 0, core), (other, k * 128, 1 - core))
        for part, at, half in parts:
            start = pl.multiple_of((k + 1) * 256 + half * 128, 128)
            weights.append(
                pltpu.make_async_copy(
                    part.at[pl.ds(at, 128)], w_ref.at[pl.ds(start, 128)], w_sem
                )
            )
        for i in range(4):
            rows.append(
                pltpu.make_async_copy(
                    pack.at[pl.ds(128, 128), pl.ds(i * 512, 512)],
                    r_ref.at[block_of(at_ref, REL[k + 1]), pl.ds(i * 128, 128)],
                    r_sem,
                )
            )
    for copy in weights + rows:
        copy.start()
    squares = jnp.zeros((8, BLK), F32)
    for k, rel in enumerate(REL):
        g_ref[:, k * 256 : (k + 1) * 256] = cells[k][0:TOK, :]
        left = cells[k][TOK : TOK + 16, 0:128].astype(F32)
        right = cells[k][TOK : TOK + 16, 128:256].astype(F32)
        squares = squares + (left[0:8, :] + right[0:8, :] + left[8:16, :])
        gain_ref[block_of(at_ref, rel)] = right[8:16, :]
    columns = jnp.transpose(lax.rsqrt(squares / 1024.0 + EPS))
    inverse = jnp.concatenate([columns[:, b : b + 1] for b in range(NB)], axis=0)
    for copy in weights + rows:
        copy.wait()

    def step(a, total):
        cols = pl.ds(pl.multiple_of(a * 512, 512), 512)
        head = jnp.dot(g_ref[...], w_ref[:, cols], preferred_element_type=F32) * inverse
        first = (r_ref[a].astype(F32) + head).astype(BF)
        r_ref[a] = first
        wide = first.astype(F32)
        return total + jnp.sum(wide * wide, axis=1, keepdims=True)

    total = lax.fori_loop(0, 4, step, jnp.zeros((TOK, 1), F32))
    own_ref[...] = r_ref[block_of(at_ref, 0)]
    inverse = lax.rsqrt(total / float(D) + EPS)

    def scale(a, carry):
        gain = gain_ref[a]
        gain = jnp.concatenate([gain[i : i + 1, :] for i in range(4)], axis=1)
        cols = pl.ds(pl.multiple_of(a * 512, 512), 512)
        normed_ref[:, cols] = (r_ref[a].astype(F32) * inverse * gain).astype(BF)
        return carry

    lax.fori_loop(0, 4, scale, 0)


def pack_kernel(at_ref, weight_ref, resid_ref, out_ref):
    start = pl.multiple_of(at_ref[2] * 128, 128)
    out_ref[0:128, :] = weight_ref[pl.ds(start, 128), :]
    for i in range(4):
        out_ref[128:256, i * 512 : (i + 1) * 512] = resid_ref[i * 128 : (i + 1) * 128, :]


def heads_kernel(a, b, c, out_ref):
    for k, ref in enumerate((a, b, c)):
        out_ref[k * 128 : (k + 1) * 128, :] = ref[0:128, :]


def pairs_kernel(own, p1, m1, a_ref, b_ref):
    a_ref[0:32, :] = own[...]
    a_ref[32:64, :] = p1[...]
    b_ref[0:32, :] = own[...]
    b_ref[32:64, :] = m1[...]


def ring_kernel(own, p1, m1, p4, a, b, out):
    for k, piece in enumerate((own, p1, m1, p4)):
        out[k * 32 : (k + 1) * 32, :] = piece[...]
    out[128:192, :] = a[...]
    out[192:256, :] = b[...]


def shard_row(at_ref, dz, dy, core):
    z, y = lax.rem(at_ref[0] + dz + 8, 8), lax.rem(at_ref[1] + dy + 4, 4)
    return pl.multiple_of((z * 8 + y * 2 + core) * 32, 32)


def wait_all(dst, sem):
    pltpu.make_async_copy(dst, dst, sem).wait()


def up_kernel(at_ref, x_ref, *refs):
    own, other = refs[:8], refs[8:11]
    sq_ref, up_ref, sems = refs[11:]
    cores = (at_ref[2], 1 - at_ref[2])

    def start(f, carry):
        cols = pl.ds(pl.multiple_of(f * 1024, 1024), 1024)
        pieces = [(piece, 0) for piece in own]
        pieces += [(other[n], 128 * k) for n, count in enumerate((5, 2, 1)) for k in range(count)]
        for n, (piece, at) in enumerate(pieces):
            dz = (0, -1, 1, -2, 2, -3, 3, 4)[n % 8]
            for k, dy in enumerate(REL):
                row = shard_row(at_ref, dz, dy, cores[n // 8])
                pltpu.make_async_copy(
                    piece.at[pl.ds(at + k * 32, 32), cols],
                    up_ref.at[f, pl.ds(row, 32)],
                    sems.at[f],
                ).start()
        return carry

    lax.fori_loop(0, 2, start, 0)

    def step(f, carry):
        @pl.when(lax.rem(f, 2) == 0)
        def _():
            wait_all(up_ref.at[f // 2], sems.at[f // 2])

        part = up_ref[f // 2, :, pl.ds(pl.multiple_of(lax.rem(f, 2) * 512, 512), 512)]
        hidden = jnp.dot(x_ref[...], part, preferred_element_type=F32)
        cols = pl.ds(pl.multiple_of(f * 512, 512), 512)
        sq_ref[:, cols] = jnp.square(jnp.maximum(hidden, 0.0)).astype(BF)
        return carry

    lax.fori_loop(0, 4, step, 0)


def down_term(sq_ref, down_ref):
    part = jnp.zeros((TOK, 512), F32)
    for f in range(4):
        cols = slice(f * 512, (f + 1) * 512)
        part = part + lax.dot_general(
            sq_ref[:, cols],
            down_ref[:, cols],
            (((1,), (1,)), ((), ())),
            preferred_element_type=F32,
        )
    return part.astype(BF)


def join_kernel(at_ref, *refs):
    far_ref, near_ref, last_ref = refs[7:]
    own, (other0, other1, other3) = refs[:4], refs[4:7]
    pieces = [(piece, 0) for piece in own]
    pieces += [(other0, 0), (other1, 0), (other1, 256), (other3, 0)]
    cores = (at_ref[2], 1 - at_ref[2])
    outs = (far_ref, near_ref.at[0], near_ref.at[1], last_ref)
    for rel, dst in zip((2, 1, -1, 0), outs):
        block = block_of(at_ref, rel)

        def step(i, carry, dst=dst, block=block):
            dz = lax.rem(block * 2 + i - at_ref[0] + 8, 8)
            slot = jnp.int32(0)
            for at, key in enumerate((0, 7, 1, 4, 6, 5, 2, 3)):
                slot = jnp.where(dz == key, at, slot)
            for n, (piece, at) in enumerate(pieces):
                y = lax.rem(at_ref[1] + REL[n % 4] + 4, 4)
                row = pl.multiple_of((i * 8 + y * 2 + cores[n // 4]) * 32, 32)
                src = pl.ds(pl.multiple_of(at + slot * 32, 32), 32)
                dst[pl.ds(row, 32), :] = piece[src, :]
            return carry

        lax.fori_loop(0, 2, step, 0)


def halves(part, low_ref, high_ref):
    low_ref[...] = part[0 : TOK // 2, :]
    high_ref[...] = part[TOK // 2 :, :]


def one_kernel(sq_ref, down_ref, low_ref, high_ref):
    halves(down_term(sq_ref, down_ref), low_ref, high_ref)


def two_kernel(sq_ref, down_ref, *refs):
    part_ref = refs[4]

    def step(k, carry):
        part_ref[k] = down_term(sq_ref, down_ref.at[k])
        return carry

    lax.fori_loop(0, 2, step, 0)
    for k in range(2):
        halves(part_ref[k], *refs[2 * k : 2 * k + 2])


def stack_kernel(*refs):
    out, at = refs[-1], 0
    for ref in refs[:-1]:
        out[at : at + ref.shape[0], :] = ref[...]
        at += ref.shape[0]


def smem():
    return pl.BlockSpec(memory_space=pltpu.SMEM)


def vmem():
    return pl.BlockSpec(memory_space=pltpu.VMEM)


def hbm():
    return pl.BlockSpec(memory_space=pl.ANY)


def shape(*dims, dtype=BF):
    return jax.ShapeDtypeStruct(dims, dtype)


def call(body, specs, outs, scratch=(), flops=0, mib=8):
    many = isinstance(outs, (list, tuple))
    return pl.pallas_call(
        body,
        in_specs=specs,
        out_specs=[vmem() for _ in outs] if many else vmem(),
        out_shape=outs,
        scratch_shapes=list(scratch),
        compiler_params=pltpu.CompilerParams(vmem_limit_bytes=mib * 1024 * 1024),
        cost_estimate=pl.CostEstimate(flops=flops, bytes_accessed=0, transcendentals=0),
    )


def local(
    queries,
    keys,
    values,
    output_gate_logits,
    input_gate_log,
    forget_gate_logits,
    extra_decay_log,
    document,
    residual,
    cell_norm_gain,
    output_weight,
    mixer_norm_gain,
    up_weight,
    down_weight,
):
    z, y, c, x = (lax.axis_index(a) for a in ("z", "y", "c", "x"))
    at = jnp.stack([z, y, c, x]).astype(jnp.int32)

    forget_log = jax.nn.log_sigmoid(forget_gate_logits) + extra_decay_log
    docs = document.astype(F32).reshape(NB, BLK)
    gates = jnp.concatenate(
        [input_gate_log.T.reshape(8, BLK), forget_log.T.reshape(8, BLK), docs, docs], axis=0
    )

    own = down_weight.T
    p1, m1 = shift(own, "z", 1), shift(own, "z", -1)
    up_y = [
        up_weight, shift(up_weight, "y", 1), shift(up_weight, "y", -1), shift(up_weight, "y", 2)
    ]

    state, numer, aux = call(
        cell_kernel,
        [vmem()] * 4,
        [shape(288, DH), shape(TOK, 256, dtype=F32), shape(TOK, BLK, dtype=F32)],
        flops=5 * 2 * 10 * 128**3,
    )(gates, queries, keys, values)
    states = [shift_sp(state, by) for by in (1, 2, 3, 4)]

    def to_all(value):
        return [shift(value, "x", by) for by in (1, -1, 2)]

    pack = call(pack_kernel, [smem()] + [vmem()] * 2, shape(256, D))(at, output_weight, residual)
    packs = to_all(pack)
    heads = call(heads_kernel, [vmem()] * 3, shape(384, D))(*packs)
    heads = shift(heads, "c", 1)

    def stack(*pieces):
        rows = sum(piece.shape[0] for piece in pieces)
        return call(stack_kernel, [vmem()] * len(pieces), shape(rows, FF), mib=16)(*pieces)

    pair = shape(64, FF)
    a2, b2 = call(pairs_kernel, [vmem()] * 3, [pair, pair])(own, p1, m1)
    a2, b2 = shift(a2, "z", 2), shift(b2, "z", -2)
    p4 = shift(own, "z", 4)
    ring = call(ring_kernel, [vmem()] * 6, shape(256, FF))(own, p1, m1, p4, a2, b2)
    downs = [ring, shift(ring, "y", 1), shift(ring, "y", -1), shift(ring, "y", 2)]
    other = [ring, stack(*downs[1:3]), downs[3]]
    downs += [shift(a, "c", 1) for a in other]

    up_rows = stack(*up_y)
    u1, d1 = shift(up_rows, "z", 1), shift(up_rows, "z", -1)
    u2, d2 = shift(u1, "z", 1), shift(d1, "z", -1)
    u3, d3 = shift(u2, "z", 1), shift(d2, "z", -1)
    ups = [up_rows, u1, d1, u2, d2, u3, d3, shift(u3, "z", 1)]
    other = [stack(*ups[:5]), stack(*ups[5:7])]
    ups += [shift(a, "c", 1) for a in (*other, ups[7])]

    cells = call(
        combine_kernel,
        [vmem()] * 11,
        shape(TOK + 16, 256),
        [pltpu.VMEM((NB, BLK, BLK), F32)],
        flops=2 * 2 * 512 * 128 * 128,
    )(
        gates,
        queries,
        output_gate_logits,
        cell_norm_gain[None, :],
        mixer_norm_gain.reshape(4, BLK),
        numer,
        aux,
        *states,
    )
    cells = [cells, *to_all(cells)]

    normed, first = call(
        project_kernel,
        [smem()] + [vmem()] * 4 + [hbm()] * 6,
        [shape(TOK, D), shape(TOK, 512)],
        [
            pltpu.VMEM((1024, D), BF),
            pltpu.VMEM((TOK, 1024), BF),
            pltpu.VMEM((4, TOK, 512), BF),
            pltpu.VMEM((4, 8, BLK), F32),
            pltpu.SemaphoreType.DMA,
            pltpu.SemaphoreType.DMA,
        ],
        flops=2 * 512 * 1024 * 2048,
        mib=24,
    )(at, *cells, residual, output_weight, *packs, heads)

    far_down, near_down, own_down = call(
        join_kernel,
        [smem()] + [vmem()] * 7,
        [shape(512, FF), shape(2, 512, FF), shape(512, FF)],
        flops=2**30,
        mib=18,
    )(at, *downs)
    squared = call(
        up_kernel,
        [smem(), vmem()] + [hbm()] * 11,
        shape(TOK, FF),
        [pltpu.VMEM((2, D, 1024), BF), pltpu.SemaphoreType.DMA((2,))],
        flops=2 * 512 * 2048 * 2048,
        mib=14,
    )(at, normed, *ups)

    half_block = shape(TOK // 2, 512)

    def one_call(down):
        return call(
            one_kernel, [vmem()] * 2, [half_block] * 2, flops=2 * 512 * 2048 * 512, mib=12
        )(squared, down)

    far_low, far_high = one_call(far_down)
    far_low, far_high = shift(far_low, "x", 1), shift(far_high, "x", -1)
    right_low, right_high, left_low, left_high = call(
        two_kernel,
        [vmem()] * 2,
        [half_block] * 4,
        [pltpu.VMEM((2, TOK, 512), BF)],
        flops=2 * 512 * 2048 * 1024,
        mib=14,
    )(squared, near_down)
    from_left_high = shift(right_high, "x", 1)
    from_right_low = shift(left_low, "x", -1)
    add = lambda a, b: (a.astype(F32) + b.astype(F32)).astype(BF)
    from_left_low = shift(add(right_low, far_low), "x", 1)
    from_right_high = shift(add(left_high, far_high), "x", -1)
    own_low, own_high = one_call(own_down)
    own_term = jnp.concatenate([own_low, own_high], axis=0)
    from_left = jnp.concatenate([from_left_low, from_left_high], axis=0)
    from_right = jnp.concatenate([from_right_low, from_right_high], axis=0)
    terms = own_term.astype(F32) + from_left.astype(F32) + from_right.astype(F32)
    return (first.astype(F32) + terms).astype(BF)


def solution(mesh):
    split = Mesh(mesh.devices.reshape(8, 4, 2, 4), ("z", "y", "c", "x"))

    return jax.shard_map(
        local,
        mesh=split,
        in_specs=(
            P(SP, "x"),
            P(SP, "x"),
            P(SP, "x"),
            P(SP, "x"),
            P(SP, "x"),
            P(SP, "x"),
            P(SP, "x"),
            P(SP),
            P(SP, "x"),
            P("x"),
            P("x", None),
            P("x"),
            P(SP, "x"),
            P("x", SP),
        ),
        out_specs=P(SP, "x"),
        check_vma=False,
    )
```

profile of v0, /device:TPU:1, one launch (start us, length us, event | category | flops | bytes accessed | tf_op | source)
XLA Modules:
  0.0 203.7 jit_solution(4841645649457266501)
XLA Ops:
  5.1 2.5 %shard_map.136 = (bf16[288,128]{1,0:T(8,128)(2,1)S(1)}, f32[512,256]{1,0:T(8,128)S(1)}, f32[512,128]{1,0:T(8,128)S(1)}) custom-call(f32[24,128]{1,0:T(8,128)S(1)} %pad_maximum_fusion.gates_ref, bf16[512,256]{1,0:T(8,128)(2,1)S(1)} %copy-done.1, bf16[512,256]{1,0:T(8,128)(2,1)S(1)} %copy-done.5, bf16[512,256]{1,0:T(8,128)(2,1)S(1)} %copy-done.6), custom_call_target="tpu_custom_call" | custom-call | flops 209715200 | tf_op jit(solution)/shard_map/pallas_call | solution.py:492
  7.6 4.6 %collective-permute-start = (bf16[288,128]{1,0:T(8,128)(2,1)S(1)}, bf16[288,128]{1,0:T(8,128)(2,1)S(1)}, u32[]{:S(2)}, u32[]{:S(2)}) collective-permute-start(bf16[288,128]{1,0:T(8,128)(2,1)S(1)} %get-tuple-element.25), channel_id=1, source_target_pairs={{0,4},{4,8},{8,12},{12,16},{16,20},{20,24},{24,28},{28,32},{32,36}... | collective-permute-start | bytes 221192 | tf_op jit(solution)/shard_map/ppermute | solution.py:32
  12.2 3.2 %collective-permute-start.1 = (bf16[288,128]{1,0:T(8,128)(2,1)S(1)}, bf16[288,128]{1,0:T(8,128)(2,1)S(1)}, u32[]{:S(2)}, u32[]{:S(2)}) collective-permute-start(bf16[288,128]{1,0:T(8,128)(2,1)S(1)} %get-tuple-element.25), channel_id=1, source_target_pairs={{0,8},{4,12},{8,16},{12,20},{16,24},{20,28},{24,32},{28,36},{32,40... | collective-permute-start | bytes 221192 | tf_op jit(solution)/shard_map/ppermute | solution.py:32
  15.4 3.5 %collective-permute-start.2 = (bf16[288,128]{1,0:T(8,128)(2,1)S(1)}, bf16[288,128]{1,0:T(8,128)(2,1)S(1)}, u32[]{:S(2)}, u32[]{:S(2)}) collective-permute-start(bf16[288,128]{1,0:T(8,128)(2,1)S(1)} %get-tuple-element.25), channel_id=1, source_target_pairs={{0,12},{4,16},{8,20},{12,24},{16,28},{20,32},{24,36},{28,40},{32,4... | collective-permute-start | bytes 221192 | tf_op jit(solution)/shard_map/ppermute | solution.py:32
  18.9 3.6 %collective-permute-start.3 = (bf16[288,128]{1,0:T(8,128)(2,1)S(1)}, bf16[288,128]{1,0:T(8,128)(2,1)S(1)}, u32[]{:S(2)}, u32[]{:S(2)}) collective-permute-start(bf16[288,128]{1,0:T(8,128)(2,1)S(1)} %get-tuple-element.25), channel_id=1, source_target_pairs={{0,16},{4,20},{8,24},{12,28},{16,32},{20,36},{24,40},{28,44},{32,4... | collective-permute-start | bytes 221192 | tf_op jit(solution)/shard_map/ppermute | solution.py:32
  28.7 2.6 %shard_map.137.refs_0_ = bf16[528,256]{1,0:T(8,128)(2,1)S(1)} custom-call(f32[24,128]{1,0:T(8,128)S(1)} %pad_maximum_fusion.gates_ref, bf16[512,256]{1,0:T(8,128)(2,1)S(1)} %copy-done.2, bf16[512,256]{1,0:T(8,128)(2,1)S(1)} %copy-done.7, bf16[1,256]{1,0:T(2,128)(2,1)S(1)} %broadcast_in_dim.3.gain_ref, bf16[4,128]{1,0:T(4,128)(2,1)S(1)} %bitcast.16, ...), custom_call_target="tpu_custom_call" | custom-call | flops 33554432 | tf_op jit(solution)/shard_map/pallas_call | solution.py:529
  32.5 2.8 %collective-permute-start.24 = (bf16[32,2048]{1,0:T(8,128)(2,1)}, bf16[32,2048]{1,0:T(8,128)(2,1)S(1)}, u32[]{:S(2)}, u32[]{:S(2)}) collective-permute-start(bf16[32,2048]{1,0:T(8,128)(2,1)} %bitcast.11), channel_id=1, source_target_pairs={{0,32},{32,64},{64,96},{96,128},{128,160},{160,192},{192,224},{224... | collective-permute-start | bytes 393224 | tf_op jit(solution)/shard_map/ppermute | solution.py:28
  35.3 3.9 %collective-permute-start.25 = (bf16[32,2048]{1,0:T(8,128)(2,1)}, bf16[32,2048]{1,0:T(8,128)(2,1)S(1)}, u32[]{:S(2)}, u32[]{:S(2)}) collective-permute-start(bf16[32,2048]{1,0:T(8,128)(2,1)} %bitcast.12), channel_id=1, source_target_pairs={{0,224},{32,0},{64,32},{96,64},{128,96},{160,128},{192,160},{224,1... | collective-permute-start | bytes 393224 | tf_op jit(solution)/shard_map/ppermute | solution.py:28
  39.3 5.3 %collective-permute-start.26 = (bf16[32,2048]{1,0:T(8,128)(2,1)}, bf16[32,2048]{1,0:T(8,128)(2,1)S(1)}, u32[]{:S(2)}, u32[]{:S(2)}) collective-permute-start(bf16[32,2048]{1,0:T(8,128)(2,1)} %bitcast.13), channel_id=1, source_target_pairs={{0,128},{32,160},{64,192},{96,224},{128,0},{160,32},{192,64},{224,... | collective-permute-start | bytes 393224 | tf_op jit(solution)/shard_map/ppermute | solution.py:28
  48.2 3.6 %collective-permute-start.28 = (bf16[64,2048]{1,0:T(8,128)(2,1)S(1)}, bf16[64,2048]{1,0:T(8,128)(2,1)S(1)}, u32[]{:S(2)}, u32[]{:S(2)}) collective-permute-start(bf16[64,2048]{1,0:T(8,128)(2,1)S(1)} %get-tuple-element.29), channel_id=1, source_target_pairs={{0,192},{32,224},{64,0},{96,32},{128,64},{160,96},{192,128},{224,1... | collective-permute-start | bytes 786440 | tf_op jit(solution)/shard_map/ppermute | solution.py:28
  51.8 3.5 %collective-permute-start.14 = (bf16[128,2048]{1,0:T(8,128)(2,1)S(1)}, bf16[128,2048]{1,0:T(8,128)(2,1)S(1)}, u32[]{:S(2)}, u32[]{:S(2)}) collective-permute-start(bf16[128,2048]{1,0:T(8,128)(2,1)S(1)} %shard_map.141.refs_0_), channel_id=1, source_target_pairs={{0,32},{32,64},{64,96},{96,128},{128,160},{160,192},{192,224},{224... | collective-permute-start | bytes 1572872 | tf_op jit(solution)/shard_map/ppermute | solution.py:28
  55.3 2.6 %collective-permute-done.27.a = bf16[64,2048]{1,0:T(8,128)(2,1)S(1)} collective-permute-done((bf16[64,2048]{1,0:T(8,128)(2,1)S(1)}, bf16[64,2048]{1,0:T(8,128)(2,1)S(1)}, u32[]{:S(2)}, u32[]{:S(2)}) %collective-permute-start.27) | collective-permute-done | bytes 262176 | tf_op jit(solution)/shard_map/ppermute | solution.py:28
  57.9 4.3 %collective-permute-start.15 = (bf16[128,2048]{1,0:T(8,128)(2,1)S(1)}, bf16[128,2048]{1,0:T(8,128)(2,1)S(1)}, u32[]{:S(2)}, u32[]{:S(2)}) collective-permute-start(bf16[128,2048]{1,0:T(8,128)(2,1)S(1)} %shard_map.141.refs_0_), channel_id=1, source_target_pairs={{0,224},{32,0},{64,32},{96,64},{128,96},{160,128},{192,160},{224,1... | collective-permute-start | bytes 1572872 | tf_op jit(solution)/shard_map/ppermute | solution.py:28
  63.3 8.1 %collective-permute-done.14.refs_1_ = bf16[128,2048]{1,0:T(8,128)(2,1)S(1)} collective-permute-done((bf16[128,2048]{1,0:T(8,128)(2,1)S(1)}, bf16[128,2048]{1,0:T(8,128)(2,1)S(1)}, u32[]{:S(2)}, u32[]{:S(2)}) %collective-permute-start.14) | collective-permute-done | bytes 524320 | tf_op jit(solution)/shard_map/ppermute | solution.py:28
  71.3 5.5 %collective-permute-start.16 = (bf16[128,2048]{1,0:T(8,128)(2,1)S(1)}, bf16[128,2048]{1,0:T(8,128)(2,1)S(1)}, u32[]{:S(2)}, u32[]{:S(2)}) collective-permute-start(bf16[128,2048]{1,0:T(8,128)(2,1)S(1)} %collective-permute-done.14.refs_1_), channel_id=1, source_target_pairs={{0,32},{32,64},{64,96},{96,128},{128,160},{160,192},{192,224},{224... | collective-permute-start | bytes 1572872 | tf_op jit(solution)/shard_map/ppermute | solution.py:28
  77.3 2.4 %collective-permute-start.30 = (bf16[256,2048]{1,0:T(8,128)(2,1)S(1)}, bf16[256,2048]{1,0:T(8,128)(2,1)S(1)}, u32[]{:S(2)}, u32[]{:S(2)}) collective-permute-start(bf16[256,2048]{1,0:T(8,128)(2,1)S(1)} %shard_map.146.refs_0_), channel_id=1, source_target_pairs={{0,24},{8,0},{16,8},{24,16},{1,25},{9,1},{17,9},{25,17},{2,26},{10... | collective-permute-start | bytes 3145736 | tf_op jit(solution)/shard_map/ppermute | solution.py:28
  81.0 6.6 %collective-permute-done.16.refs_3_ = bf16[128,2048]{1,0:T(8,128)(2,1)S(1)} collective-permute-done((bf16[128,2048]{1,0:T(8,128)(2,1)S(1)}, bf16[128,2048]{1,0:T(8,128)(2,1)S(1)}, u32[]{:S(2)}, u32[]{:S(2)}) %collective-permute-start.16) | collective-permute-done | bytes 524320 | tf_op jit(solution)/shard_map/ppermute | solution.py:28
  87.6 5.2 %collective-permute-done.17.refs_4_ = bf16[128,2048]{1,0:T(8,128)(2,1)S(1)} collective-permute-done((bf16[128,2048]{1,0:T(8,128)(2,1)S(1)}, bf16[128,2048]{1,0:T(8,128)(2,1)S(1)}, u32[]{:S(2)}, u32[]{:S(2)}) %collective-permute-start.17) | collective-permute-done | bytes 524320 | tf_op jit(solution)/shard_map/ppermute | solution.py:28
  94.9 29.5 %collective-permute-done.29.refs_0_.refs_1_ = bf16[256,2048]{1,0:T(8,128)(2,1)S(1)} collective-permute-done((bf16[256,2048]{1,0:T(8,128)(2,1)S(1)}, bf16[256,2048]{1,0:T(8,128)(2,1)S(1)}, u32[]{:S(2)}, u32[]{:S(2)}) %collective-permute-start.29) | collective-permute-done | bytes 1048608 | tf_op jit(solution)/shard_map/ppermute | solution.py:28
  128.1 7.7 %collective-permute-done.6.refs_3_ = bf16[528,256]{1,0:T(8,128)(2,1)S(1)} collective-permute-done((bf16[528,256]{1,0:T(8,128)(2,1)S(1)}, bf16[528,256]{1,0:T(8,128)(2,1)S(1)}, u32[]{:S(2)}, u32[]{:S(2)}) %collective-permute-start.6) | collective-permute-done | bytes 270368 | tf_op jit(solution)/shard_map/ppermute | solution.py:28
  135.8 2.2 %collective-permute-start.18 = (bf16[128,2048]{1,0:T(8,128)(2,1)S(1)}, bf16[128,2048]{1,0:T(8,128)(2,1)S(1)}, u32[]{:S(2)}, u32[]{:S(2)}) collective-permute-start(bf16[128,2048]{1,0:T(8,128)(2,1)S(1)} %collective-permute-done.16.refs_3_), channel_id=1, source_target_pairs={{0,32},{32,64},{64,96},{96,128},{128,160},{160,192},{192,224},{224... | collective-permute-start | bytes 1572872 | tf_op jit(solution)/shard_map/ppermute | solution.py:28
  139.6 10.0 %collective-permute-done.18.refs_0_.refs_5_ = bf16[128,2048]{1,0:T(8,128)(2,1)S(1)} collective-permute-done((bf16[128,2048]{1,0:T(8,128)(2,1)S(1)}, bf16[128,2048]{1,0:T(8,128)(2,1)S(1)}, u32[]{:S(2)}, u32[]{:S(2)}) %collective-permute-start.18) | collective-permute-done | bytes 524320 | tf_op jit(solution)/shard_map/ppermute | solution.py:28
  150.6 1.9 collective-permute-done.19.refs_1_.refs_6_
  153.5 9.0 %collective-permute-done.20.refs_7_ = bf16[128,2048]{1,0:T(8,128)(2,1)S(1)} collective-permute-done((bf16[128,2048]{1,0:T(8,128)(2,1)S(1)}, bf16[128,2048]{1,0:T(8,128)(2,1)S(1)}, u32[]{:S(2)}, u32[]{:S(2)}) %collective-permute-start.20) | collective-permute-done | bytes 524320 | tf_op jit(solution)/shard_map/ppermute | solution.py:28
  162.6 2.6 %collective-permute-start.22 = (bf16[256,2048]{1,0:T(8,128)(2,1)S(1)}, bf16[256,2048]{1,0:T(8,128)(2,1)S(1)}, u32[]{:S(2)}, u32[]{:S(2)}) collective-permute-start(bf16[256,2048]{1,0:T(8,128)(2,1)S(1)} %shard_map.143), channel_id=1, source_target_pairs={{0,4},{4,0},{1,5},{5,1},{2,6},{6,2},{3,7},{7,3},{8,12},{12,8},{9,1... | collective-permute-start | bytes 3145736 | tf_op jit(solution)/shard_map/ppermute | solution.py:28
  165.2 5.5 %shard_map.140 = (bf16[512,2048]{1,0:T(8,128)(2,1)S(1)}, bf16[512,512]{1,0:T(8,128)(2,1)S(1)}) custom-call(s32[4]{0:T(128)S(1)} %pad_add_fusion.at_ref, bf16[528,256]{1,0:T(8,128)(2,1)S(1)} %shard_map.137.refs_0_, bf16[528,256]{1,0:T(8,128)(2,1)S(1)} %collective-permute-done.4.refs_1_, bf16[528,256]{1,0:T(8,128)(2,1)S(1)} %collective-permute-done.5.refs_2_, ...), custom_call_target="tpu_custom_call" | custom-call | flops 2147483648 | tf_op jit(solution)/shard_map/pallas_call | solution.py:547
  172.1 9.7 %shard_map.144.sq_ref = bf16[512,2048]{1,0:T(8,128)(2,1)S(1)} custom-call(s32[4]{0:T(128)S(1)} %pad_add_fusion.at_ref, bf16[512,2048]{1,0:T(8,128)(2,1)S(1)} %get-tuple-element.27.x_ref, bf16[128,2048]{1,0:T(8,128)(2,1)S(1)} %shard_map.141.refs_0_, bf16[128,2048]{1,0:T(8,128)(2,1)S(1)} %collective-permute-done.14.refs_1_, ...), custom_call_target="tpu_custom_call" | custom-call | flops 4294967296 | tf_op jit(solution)/shard_map/pallas_call | solution.py:570
  183.1 2.7 %collective-permute-start.39 = (bf16[256,512]{1,0:T(8,128)(2,1)S(1)}, bf16[256,512]{1,0:T(8,128)(2,1)S(1)}, u32[]{:S(2)}, u32[]{:S(2)}) collective-permute-start(bf16[256,512]{1,0:T(8,128)(2,1)S(1)} %get-tuple-element.40), channel_id=1, source_target_pairs={{0,3},{1,0},{2,1},{3,2},{4,7},{5,4},{6,5},{7,6},{8,11},{9,8},{10,9... | collective-permute-start | bytes 786440 | tf_op jit(solution)/shard_map/ppermute | solution.py:28
  185.8 2.6 %shard_map.150 = (bf16[256,512]{1,0:T(8,128)(2,1)S(1)}, bf16[256,512]{1,0:T(8,128)(2,1)S(1)}, bf16[256,512]{1,0:T(8,128)(2,1)S(1)}, bf16[256,512]{1,0:T(8,128)(2,1)S(1)}) custom-call(bf16[512,2048]{1,0:T(8,128)(2,1)S(1)} %shard_map.144.sq_ref, bf16[2,512,2048]{2,1,0:T(8,128)(2,1)S(1)} %get-tuple-element.33.down_ref), custom_call_target="tpu_custom_call" | custom-call | flops 2147483648 | tf_op jit(solution)/shard_map/pallas_call | solution.py:588
  188.5 2.7 %collective-permute-start.38 = (bf16[256,512]{1,0:T(8,128)(2,1)S(1)}, bf16[256,512]{1,0:T(8,128)(2,1)S(1)}, u32[]{:S(2)}, u32[]{:S(2)}) collective-permute-start(bf16[256,512]{1,0:T(8,128)(2,1)S(1)} %get-tuple-element.38), channel_id=1, source_target_pairs={{0,3},{1,0},{2,1},{3,2},{4,7},{5,4},{6,5},{7,6},{8,11},{9,8},{10,9... | collective-permute-start | bytes 786440 | tf_op jit(solution)/shard_map/ppermute | solution.py:28
  191.9 2.7 %collective-permute-start.40 = (bf16[256,512]{1,0:T(8,128)(2,1)S(1)}, bf16[256,512]{1,0:T(8,128)(2,1)S(1)}, u32[]{:S(2)}, u32[]{:S(2)}) collective-permute-start(bf16[256,512]{1,0:T(8,128)(2,1)S(1)} %add_convert_fusion.1), channel_id=1, source_target_pairs={{0,3},{1,0},{2,1},{3,2},{4,7},{5,4},{6,5},{7,6},{8,11},{9,8},{10,9... | collective-permute-start | bytes 786440 | tf_op jit(solution)/shard_map/ppermute | solution.py:28
  197.0 5.6 %collective-permute-done.36 = bf16[256,512]{1,0:T(8,128)(2,1)S(1)} collective-permute-done((bf16[256,512]{1,0:T(8,128)(2,1)S(1)}, bf16[256,512]{1,0:T(8,128)(2,1)S(1)}, u32[]{:S(2)}, u32[]{:S(2)}) %collective-permute-start.36) | collective-permute-done | bytes 262176 | tf_op jit(solution)/shard_map/ppermute | solution.py:28
  (96 shorter events, 35.2 us)
Async XLA Ops:
  7.6 16.3 %collective-permute-start = (bf16[288,128]{1,0:T(8,128)(2,1)S(1)}, bf16[288,128]{1,0:T(8,128)(2,1)S(1)}, u32[]{:S(2)}, u32[]{:S(2)}) collective-permute-start(bf16[288,128]{1,0:T(8,128)(2,1)S(1)} %get-tuple-element.25), channel_id=1, source_target_pairs={{0,4},{4,8},{8,12},{12,16},{16,20},{20,24},{24,28},{28,32},{32,36}... | collective-permute-start | bytes 221192 | tf_op jit(solution)/shard_map/ppermute | solution.py:32
  12.2 13.9 %collective-permute-start.1 = (bf16[288,128]{1,0:T(8,128)(2,1)S(1)}, bf16[288,128]{1,0:T(8,128)(2,1)S(1)}, u32[]{:S(2)}, u32[]{:S(2)}) collective-permute-start(bf16[288,128]{1,0:T(8,128)(2,1)S(1)} %get-tuple-element.25), channel_id=1, source_target_pairs={{0,8},{4,12},{8,16},{12,20},{16,24},{20,28},{24,32},{28,36},{32,40... | collective-permute-start | bytes 221192 | tf_op jit(solution)/shard_map/ppermute | solution.py:32
  15.4 10.7 %collective-permute-start.2 = (bf16[288,128]{1,0:T(8,128)(2,1)S(1)}, bf16[288,128]{1,0:T(8,128)(2,1)S(1)}, u32[]{:S(2)}, u32[]{:S(2)}) collective-permute-start(bf16[288,128]{1,0:T(8,128)(2,1)S(1)} %get-tuple-element.25), channel_id=1, source_target_pairs={{0,12},{4,16},{8,20},{12,24},{16,28},{20,32},{24,36},{28,40},{32,4... | collective-permute-start | bytes 221192 | tf_op jit(solution)/shard_map/ppermute | solution.py:32
  22.5 16.7 %collective-permute-start.11 = (bf16[32,2048]{1,0:T(8,128)(2,1)}, bf16[32,2048]{1,0:T(8,128)(2,1)S(1)}, u32[]{:S(2)}, u32[]{:S(2)}) collective-permute-start(bf16[32,2048]{1,0:T(8,128)(2,1)} %refs_0_.1), channel_id=1, source_target_pairs={{0,8},{8,16},{16,24},{24,0},{1,9},{9,17},{17,25},{25,1},{2,10},{10... | collective-permute-start | bytes 393224 | tf_op jit(solution)/shard_map/ppermute | solution.py:28
  23.9 15.4 %collective-permute-start.12 = (bf16[32,2048]{1,0:T(8,128)(2,1)}, bf16[32,2048]{1,0:T(8,128)(2,1)S(1)}, u32[]{:S(2)}, u32[]{:S(2)}) collective-permute-start(bf16[32,2048]{1,0:T(8,128)(2,1)} %refs_0_.1), channel_id=1, source_target_pairs={{0,24},{8,0},{16,8},{24,16},{1,25},{9,1},{17,9},{25,17},{2,26},{10... | collective-permute-start | bytes 393224 | tf_op jit(solution)/shard_map/ppermute | solution.py:28
  31.3 20.5 %collective-permute-start.4 = (bf16[528,256]{1,0:T(8,128)(2,1)S(1)}, bf16[528,256]{1,0:T(8,128)(2,1)S(1)}, u32[]{:S(2)}, u32[]{:S(2)}) collective-permute-start(bf16[528,256]{1,0:T(8,128)(2,1)S(1)} %shard_map.137.refs_0_), channel_id=1, source_target_pairs={{0,1},{1,2},{2,3},{3,0},{4,5},{5,6},{6,7},{7,4},{8,9},{9,10},{10,1... | collective-permute-start | bytes 811016 | tf_op jit(solution)/shard_map/ppermute | solution.py:28
  32.5 12.7 %collective-permute-start.24 = (bf16[32,2048]{1,0:T(8,128)(2,1)}, bf16[32,2048]{1,0:T(8,128)(2,1)S(1)}, u32[]{:S(2)}, u32[]{:S(2)}) collective-permute-start(bf16[32,2048]{1,0:T(8,128)(2,1)} %bitcast.11), channel_id=1, source_target_pairs={{0,32},{32,64},{64,96},{96,128},{128,160},{160,192},{192,224},{224... | collective-permute-start | bytes 393224 | tf_op jit(solution)/shard_map/ppermute | solution.py:28
  35.3 11.3 %collective-permute-start.25 = (bf16[32,2048]{1,0:T(8,128)(2,1)}, bf16[32,2048]{1,0:T(8,128)(2,1)S(1)}, u32[]{:S(2)}, u32[]{:S(2)}) collective-permute-start(bf16[32,2048]{1,0:T(8,128)(2,1)} %bitcast.12), channel_id=1, source_target_pairs={{0,224},{32,0},{64,32},{96,64},{128,96},{160,128},{192,160},{224,1... | collective-permute-start | bytes 393224 | tf_op jit(solution)/shard_map/ppermute | solution.py:28
  45.3 34.4 %collective-permute-start.7 = (bf16[256,2048]{1,0:T(8,128)(2,1)S(1)}, bf16[256,2048]{1,0:T(8,128)(2,1)S(1)}, u32[]{:S(2)}, u32[]{:S(2)}) collective-permute-start(bf16[256,2048]{1,0:T(8,128)(2,1)S(1)} %shard_map.138), channel_id=1, source_target_pairs={{0,1},{1,2},{2,3},{3,0},{4,5},{5,6},{6,7},{7,4},{8,9},{9,10},{10,1... | collective-permute-start | bytes 3145736 | tf_op jit(solution)/shard_map/ppermute | solution.py:28
  46.6 33.1 %collective-permute-start.8 = (bf16[256,2048]{1,0:T(8,128)(2,1)S(1)}, bf16[256,2048]{1,0:T(8,128)(2,1)S(1)}, u32[]{:S(2)}, u32[]{:S(2)}) collective-permute-start(bf16[256,2048]{1,0:T(8,128)(2,1)S(1)} %shard_map.138), channel_id=1, source_target_pairs={{0,3},{1,0},{2,1},{3,2},{4,7},{5,4},{6,5},{7,6},{8,11},{9,8},{10,9... | collective-permute-start | bytes 3145736 | tf_op jit(solution)/shard_map/ppermute | solution.py:28
  48.1 9.8 %collective-permute-start.27 = (bf16[64,2048]{1,0:T(8,128)(2,1)S(1)}, bf16[64,2048]{1,0:T(8,128)(2,1)S(1)}, u32[]{:S(2)}, u32[]{:S(2)}) collective-permute-start(bf16[64,2048]{1,0:T(8,128)(2,1)S(1)} %get-tuple-element.28), channel_id=1, source_target_pairs={{0,64},{32,96},{64,128},{96,160},{128,192},{160,224},{192,0},{224,... | collective-permute-start | bytes 786440 | tf_op jit(solution)/shard_map/ppermute | solution.py:28
  48.2 14.0 %collective-permute-start.28 = (bf16[64,2048]{1,0:T(8,128)(2,1)S(1)}, bf16[64,2048]{1,0:T(8,128)(2,1)S(1)}, u32[]{:S(2)}, u32[]{:S(2)}) collective-permute-start(bf16[64,2048]{1,0:T(8,128)(2,1)S(1)} %get-tuple-element.29), channel_id=1, source_target_pairs={{0,192},{32,224},{64,0},{96,32},{128,64},{160,96},{192,128},{224,1... | collective-permute-start | bytes 786440 | tf_op jit(solution)/shard_map/ppermute | solution.py:28
  51.8 19.5 %collective-permute-start.14 = (bf16[128,2048]{1,0:T(8,128)(2,1)S(1)}, bf16[128,2048]{1,0:T(8,128)(2,1)S(1)}, u32[]{:S(2)}, u32[]{:S(2)}) collective-permute-start(bf16[128,2048]{1,0:T(8,128)(2,1)S(1)} %shard_map.141.refs_0_), channel_id=1, source_target_pairs={{0,32},{32,64},{64,96},{96,128},{128,160},{160,192},{192,224},{224... | collective-permute-start | bytes 1572872 | tf_op jit(solution)/shard_map/ppermute | solution.py:28
  57.9 19.4 %collective-permute-start.15 = (bf16[128,2048]{1,0:T(8,128)(2,1)S(1)}, bf16[128,2048]{1,0:T(8,128)(2,1)S(1)}, u32[]{:S(2)}, u32[]{:S(2)}) collective-permute-start(bf16[128,2048]{1,0:T(8,128)(2,1)S(1)} %shard_map.141.refs_0_), channel_id=1, source_target_pairs={{0,224},{32,0},{64,32},{96,64},{128,96},{160,128},{192,160},{224,1... | collective-permute-start | bytes 1572872 | tf_op jit(solution)/shard_map/ppermute | solution.py:28
  62.2 14.7 %collective-permute-start.5 = (bf16[528,256]{1,0:T(8,128)(2,1)S(1)}, bf16[528,256]{1,0:T(8,128)(2,1)S(1)}, u32[]{:S(2)}, u32[]{:S(2)}) collective-permute-start(bf16[528,256]{1,0:T(8,128)(2,1)S(1)} %shard_map.137.refs_0_), channel_id=1, source_target_pairs={{0,3},{1,0},{2,1},{3,2},{4,7},{5,4},{6,5},{7,6},{8,11},{9,8},{10,9... | collective-permute-start | bytes 811016 | tf_op jit(solution)/shard_map/ppermute | solution.py:28
  71.3 16.2 %collective-permute-start.16 = (bf16[128,2048]{1,0:T(8,128)(2,1)S(1)}, bf16[128,2048]{1,0:T(8,128)(2,1)S(1)}, u32[]{:S(2)}, u32[]{:S(2)}) collective-permute-start(bf16[128,2048]{1,0:T(8,128)(2,1)S(1)} %collective-permute-done.14.refs_1_), channel_id=1, source_target_pairs={{0,32},{32,64},{64,96},{96,128},{128,160},{160,192},{192,224},{224... | collective-permute-start | bytes 1572872 | tf_op jit(solution)/shard_map/ppermute | solution.py:28
  76.9 47.5 %collective-permute-start.29 = (bf16[256,2048]{1,0:T(8,128)(2,1)S(1)}, bf16[256,2048]{1,0:T(8,128)(2,1)S(1)}, u32[]{:S(2)}, u32[]{:S(2)}) collective-permute-start(bf16[256,2048]{1,0:T(8,128)(2,1)S(1)} %shard_map.146.refs_0_), channel_id=1, source_target_pairs={{0,8},{8,16},{16,24},{24,0},{1,9},{9,17},{17,25},{25,1},{2,10},{10... | collective-permute-start | bytes 3145736 | tf_op jit(solution)/shard_map/ppermute | solution.py:28
  77.3 48.9 %collective-permute-start.30 = (bf16[256,2048]{1,0:T(8,128)(2,1)S(1)}, bf16[256,2048]{1,0:T(8,128)(2,1)S(1)}, u32[]{:S(2)}, u32[]{:S(2)}) collective-permute-start(bf16[256,2048]{1,0:T(8,128)(2,1)S(1)} %shard_map.146.refs_0_), channel_id=1, source_target_pairs={{0,24},{8,0},{16,8},{24,16},{1,25},{9,1},{17,9},{25,17},{2,26},{10... | collective-permute-start | bytes 3145736 | tf_op jit(solution)/shard_map/ppermute | solution.py:28
  79.6 13.2 %collective-permute-start.17 = (bf16[128,2048]{1,0:T(8,128)(2,1)S(1)}, bf16[128,2048]{1,0:T(8,128)(2,1)S(1)}, u32[]{:S(2)}, u32[]{:S(2)}) collective-permute-start(bf16[128,2048]{1,0:T(8,128)(2,1)S(1)} %collective-permute-done.15.refs_2_), channel_id=1, source_target_pairs={{0,224},{32,0},{64,32},{96,64},{128,96},{160,128},{192,160},{224,1... | collective-permute-start | bytes 1572872 | tf_op jit(solution)/shard_map/ppermute | solution.py:28
  79.7 47.9 %collective-permute-start.9 = (bf16[256,2048]{1,0:T(8,128)(2,1)S(1)}, bf16[256,2048]{1,0:T(8,128)(2,1)S(1)}, u32[]{:S(2)}, u32[]{:S(2)}) collective-permute-start(bf16[256,2048]{1,0:T(8,128)(2,1)S(1)} %shard_map.138), channel_id=1, source_target_pairs={{0,2},{1,3},{2,0},{3,1},{4,6},{5,7},{6,4},{7,5},{8,10},{9,11},{10,... | collective-permute-start | bytes 3145736 | tf_op jit(solution)/shard_map/ppermute | solution.py:28
  87.6 50.4 %collective-permute-start.31 = (bf16[256,2048]{1,0:T(8,128)(2,1)S(1)}, bf16[256,2048]{1,0:T(8,128)(2,1)S(1)}, u32[]{:S(2)}, u32[]{:S(2)}) collective-permute-start(bf16[256,2048]{1,0:T(8,128)(2,1)S(1)} %shard_map.146.refs_0_), channel_id=1, source_target_pairs={{0,16},{8,24},{16,0},{24,8},{1,17},{9,25},{17,1},{25,9},{2,18},{10... | collective-permute-start | bytes 3145736 | tf_op jit(solution)/shard_map/ppermute | solution.py:28
  92.8 46.3 %collective-permute-start.32 = (bf16[256,2048]{1,0:T(8,128)(2,1)S(1)}, bf16[256,2048]{1,0:T(8,128)(2,1)S(1)}, u32[]{:S(2)}, u32[]{:S(2)}) collective-permute-start(bf16[256,2048]{1,0:T(8,128)(2,1)S(1)} %shard_map.146.refs_0_), channel_id=1, source_target_pairs={{0,4},{4,0},{1,5},{5,1},{2,6},{6,2},{3,7},{7,3},{8,12},{12,8},{9,1... | collective-permute-start | bytes 3145736 | tf_op jit(solution)/shard_map/ppermute | solution.py:28
  124.4 47.7 %collective-permute-start.21 = (bf16[640,2048]{1,0:T(8,128)(2,1)S(1)}, bf16[640,2048]{1,0:T(8,128)(2,1)S(1)}, u32[]{:S(2)}, u32[]{:S(2)}) collective-permute-start(bf16[640,2048]{1,0:T(8,128)(2,1)S(1)} %shard_map.142), channel_id=1, source_target_pairs={{0,4},{4,0},{1,5},{5,1},{2,6},{6,2},{3,7},{7,3},{8,12},{12,8},{9,1... | collective-permute-start | bytes 7864328 | tf_op jit(solution)/shard_map/ppermute | solution.py:28
  126.2 9.5 %collective-permute-start.6 = (bf16[528,256]{1,0:T(8,128)(2,1)S(1)}, bf16[528,256]{1,0:T(8,128)(2,1)S(1)}, u32[]{:S(2)}, u32[]{:S(2)}) collective-permute-start(bf16[528,256]{1,0:T(8,128)(2,1)S(1)} %shard_map.137.refs_0_), channel_id=1, source_target_pairs={{0,2},{1,3},{2,0},{3,1},{4,6},{5,7},{6,4},{7,5},{8,10},{9,11},{10,... | collective-permute-start | bytes 811016 | tf_op jit(solution)/shard_map/ppermute | solution.py:28
  127.6 43.1 %collective-permute-start.33 = (bf16[512,2048]{1,0:T(8,128)(2,1)S(1)}, bf16[512,2048]{1,0:T(8,128)(2,1)S(1)}, u32[]{:S(2)}, u32[]{:S(2)}) collective-permute-start(bf16[512,2048]{1,0:T(8,128)(2,1)S(1)} %shard_map.147), channel_id=1, source_target_pairs={{0,4},{4,0},{1,5},{5,1},{2,6},{6,2},{3,7},{7,3},{8,12},{12,8},{9,1... | collective-permute-start | bytes 6291464 | tf_op jit(solution)/shard_map/ppermute | solution.py:28
  135.8 13.8 %collective-permute-start.18 = (bf16[128,2048]{1,0:T(8,128)(2,1)S(1)}, bf16[128,2048]{1,0:T(8,128)(2,1)S(1)}, u32[]{:S(2)}, u32[]{:S(2)}) collective-permute-start(bf16[128,2048]{1,0:T(8,128)(2,1)S(1)} %collective-permute-done.16.refs_3_), channel_id=1, source_target_pairs={{0,32},{32,64},{64,96},{96,128},{128,160},{160,192},{192,224},{224... | collective-permute-start | bytes 1572872 | tf_op jit(solution)/shard_map/ppermute | solution.py:28
  138.0 27.2 %collective-permute-start.10 = (bf16[384,2048]{1,0:T(8,128)(2,1)S(1)}, bf16[384,2048]{1,0:T(8,128)(2,1)S(1)}, u32[]{:S(2)}, u32[]{:S(2)}) collective-permute-start(bf16[384,2048]{1,0:T(8,128)(2,1)S(1)} %shard_map.139), channel_id=1, source_target_pairs={{0,4},{4,0},{1,5},{5,1},{2,6},{6,2},{3,7},{7,3},{8,12},{12,8},{9,1... | collective-permute-start | bytes 4718600 | tf_op jit(solution)/shard_map/ppermute | solution.py:28
  139.1 13.4 %collective-permute-start.19 = (bf16[128,2048]{1,0:T(8,128)(2,1)S(1)}, bf16[128,2048]{1,0:T(8,128)(2,1)S(1)}, u32[]{:S(2)}, u32[]{:S(2)}) collective-permute-start(bf16[128,2048]{1,0:T(8,128)(2,1)S(1)} %collective-permute-done.17.refs_4_), channel_id=1, source_target_pairs={{0,224},{32,0},{64,32},{96,64},{128,96},{160,128},{192,160},{224,1... | collective-permute-start | bytes 1572872 | tf_op jit(solution)/shard_map/ppermute | solution.py:28
  149.6 13.0 %collective-permute-start.20 = (bf16[128,2048]{1,0:T(8,128)(2,1)S(1)}, bf16[128,2048]{1,0:T(8,128)(2,1)S(1)}, u32[]{:S(2)}, u32[]{:S(2)}) collective-permute-start(bf16[128,2048]{1,0:T(8,128)(2,1)S(1)} %collective-permute-done.18.refs_0_.refs_5_), channel_id=1, source_target_pairs={{0,32},{32,64},{64,96},{96,128},{128,160},{160,192},{192,224},{224... | collective-permute-start | bytes 1572872 | tf_op jit(solution)/shard_map/ppermute | solution.py:28
  152.5 18.2 %collective-permute-start.34 = (bf16[256,2048]{1,0:T(8,128)(2,1)S(1)}, bf16[256,2048]{1,0:T(8,128)(2,1)S(1)}, u32[]{:S(2)}, u32[]{:S(2)}) collective-permute-start(bf16[256,2048]{1,0:T(8,128)(2,1)S(1)} %collective-permute-done.31.refs_3_), channel_id=1, source_target_pairs={{0,4},{4,0},{1,5},{5,1},{2,6},{6,2},{3,7},{7,3},{8,12},{12,8},{9,1... | collective-permute-start | bytes 3145736 | tf_op jit(solution)/shard_map/ppermute | solution.py:28
  191.8 10.8 %collective-permute-start.36 = (bf16[256,512]{1,0:T(8,128)(2,1)S(1)}, bf16[256,512]{1,0:T(8,128)(2,1)S(1)}, u32[]{:S(2)}, u32[]{:S(2)}) collective-permute-start(bf16[256,512]{1,0:T(8,128)(2,1)S(1)} %add_convert_fusion.2), channel_id=1, source_target_pairs={{0,1},{1,2},{2,3},{3,0},{4,5},{5,6},{6,7},{7,4},{8,9},{9,10},{10,1... | collective-permute-start | bytes 786440 | tf_op jit(solution)/shard_map/ppermute | solution.py:28
  191.9 10.7 %collective-permute-start.40 = (bf16[256,512]{1,0:T(8,128)(2,1)S(1)}, bf16[256,512]{1,0:T(8,128)(2,1)S(1)}, u32[]{:S(2)}, u32[]{:S(2)}) collective-permute-start(bf16[256,512]{1,0:T(8,128)(2,1)S(1)} %add_convert_fusion.1), channel_id=1, source_target_pairs={{0,3},{1,0},{2,1},{3,2},{4,7},{5,4},{6,5},{7,6},{8,11},{9,8},{10,9... | collective-permute-start | bytes 786440 | tf_op jit(solution)/shard_map/ppermute | solution.py:28
  (19 other events, 184.0 us)
where the time goes:
time: 204 us
  waiting for transfers between devices  88.1 us (43%)
  starting transfers between devices  77.6 us (38%)
  Pallas kernels  28 us (14%)
  local copies, waits for them, and re-layouts  6.8 us (3%)
  other arithmetic  2.79 us (1%)
    ppermute x37, waiting for transfers between devices, shift(): lax.ppermute(value, axis, [(i, (i + by) % count) for i in range(count)])  88.1 us
    ppermute x37, starting transfers between devices, shift(): lax.ppermute(value, axis, [(i, (i + by) % count) for i in range(count)])  62.7 us
    ppermute x4, starting transfers between devices, shift_sp(): return lax.ppermute(value, SP, [(i, i + by) for i in range(64 - by)])  14.9 us
    pallas_call x1, Pallas kernels, local(): call(up_kernel, [smem(), vmem()] + [hbm()] * 11, shape(TOK, FF), [pltpu.V...  9.68 us
    pallas_call x1, Pallas kernels, local(): call(project_kernel, [smem()] + [vmem()] * 4 + [hbm()] * 6, [shape(TOK, D...  5.55 us
    unnamed x20, local copies, waits for them, and re-layouts  5.43 us
  transfers between devices with their start and end apart: 41, of which 13 were waited for; matrix products, arithmetic and copies ran while one was open for 0% of the time, Pallas kernels for 7%

commit v1 on v0

--- a/solution.py
+++ b/solution.py
@@ -332,22 +332,23 @@
     sq_ref, up_ref, sems = refs[11:]
     cores = (at_ref[2], 1 - at_ref[2])
 
-    def start(f, carry):
+    pieces = [(piece, 0) for piece in own]
+    pieces += [(other[n], 128 * k) for n, count in enumerate((5, 2, 1)) for k in range(count)]
+
+    def start(n, carry):
+        f, k = n // 4, lax.rem(n, 4)
         cols = pl.ds(pl.multiple_of(f * 1024, 1024), 1024)
-        pieces = [(piece, 0) for piece in own]
-        pieces += [(other[n], 128 * k) for n, count in enumerate((5, 2, 1)) for k in range(count)]
-        for n, (piece, at) in enumerate(pieces):
-            dz = (0, -1, 1, -2, 2, -3, 3, 4)[n % 8]
-            for k, dy in enumerate(REL):
-                row = shard_row(at_ref, dz, dy, cores[n // 8])
-                pltpu.make_async_copy(
-                    piece.at[pl.ds(at + k * 32, 32), cols],
-                    up_ref.at[f, pl.ds(row, 32)],
-                    sems.at[f],
-                ).start()
+        dy = jnp.where(k == 0, 0, jnp.where(k == 1, -1, k - 1))
+        for i, (piece, at) in enumerate(pieces):
+            row = shard_row(at_ref, (0, -1, 1, -2, 2, -3, 3, 4)[i % 8], dy, cores[i // 8])
+            pltpu.make_async_copy(
+                piece.at[pl.ds(pl.multiple_of(at + k * 32, 32), 32), cols],
+                up_ref.at[f, pl.ds(row, 32)],
+                sems.at[f],
+            ).start()
         return carry
 
-    lax.fori_loop(0, 2, start, 0)
+    lax.fori_loop(0, 8, start, 0)
 
     def step(f, carry):
         @pl.when(lax.rem(f, 2) == 0)
@@ -377,10 +378,10 @@
 
 
 def join_kernel(at_ref, *refs):
-    far_ref, near_ref, last_ref = refs[7:]
-    own, (other0, other1, other3) = refs[:4], refs[4:7]
+    far_ref, near_ref, last_ref = refs[6:]
+    own, (other, other_far) = refs[:4], refs[4:6]
     pieces = [(piece, 0) for piece in own]
-    pieces += [(other0, 0), (other1, 0), (other1, 256), (other3, 0)]
+    pieces += [(other, 0), (other, 256), (other, 512), (other_far, 0)]
     cores = (at_ref[2], 1 - at_ref[2])
     outs = (far_ref, near_ref.at[0], near_ref.at[1], last_ref)
     for rel, dst in zip((2, 1, -1, 0), outs):
@@ -514,8 +515,10 @@
     a2, b2 = shift(a2, "z", 2), shift(b2, "z", -2)
     p4 = shift(own, "z", 4)
     ring = call(ring_kernel, [vmem()] * 6, shape(256, FF))(own, p1, m1, p4, a2, b2)
-    downs = [ring, shift(ring, "y", 1), shift(ring, "y", -1), shift(ring, "y", 2)]
-    other = [ring, stack(*downs[1:3]), downs[3]]
+    downs = [ring, shift(ring, "y", 1), shift(ring, "y", -1)]
+    far = shift(downs[1][:128], "y", 1), shift(downs[2][128:], "y", -1)
+    downs += [stack(*far)]
+    other = [stack(*downs[:3]), downs[3]]
     downs += [shift(a, "c", 1) for a in other]
 
     up_rows = stack(*up_y)
@@ -562,7 +565,7 @@
 
     far_down, near_down, own_down = call(
         join_kernel,
-        [smem()] + [vmem()] * 7,
+        [smem()] + [vmem()] * 6,
         [shape(512, FF), shape(2, 512, FF), shape(512, FF)],
         flops=2**30,
         mib=18,

time: 204 us -> 221 us (1.083)
  starting transfers between devices: 77.6 us -> 84.9 us
  waiting for transfers between devices: 88.1 us -> 93 us
  Pallas kernels: 28 us -> 32.8 us
    ppermute x4, starting transfers between devices: 14.9 us -> 23 us  [shift_sp(): return lax.ppermute(value, SP, [(i, i + by) for i in range(64 - by)])]
    ppermute x4, waiting for transfers between devices: 0.01 us -> 5.17 us  [shift_sp(): return lax.ppermute(value, SP, [(i, i + by) for i in range(64 - by)])]
    pallas_call x4 -> x5, Pallas kernels: 0.41 us -> 2.87 us  [stack(): call(stack_kernel, [vmem()] * len(pieces), shape(rows, FF), mib=16)(*pieces)]
    unnamed x20 -> x42, local copies, waits for them, and re-layouts: 5.43 us -> 7.24 us
  transfers between devices with their start and end apart: 41 -> 41, of which waited for: 13 -> 19; matrix products, arithmetic and copies ran while one was open for 0% -> 0% of each run, Pallas kernels for 7% -> 14%
where the time goes in v1:
time: 221 us; the launch traced here: 220 us
  waiting for transfers between devices  93 us (42%)
  starting transfers between devices  84.9 us (38%)
  Pallas kernels  32.8 us (15%)
  local copies, waits for them, and re-layouts  7.33 us (3%)
    ppermute x37, waiting for transfers between devices, shift(): lax.ppermute(value, axis, [(i, (i + by) % count) for i in range(count)])  87.9 us
    ppermute x37, starting transfers between devices, shift(): lax.ppermute(value, axis, [(i, (i + by) % count) for i in range(count)])  61.9 us
    ppermute x4, starting transfers between devices, shift_sp(): return lax.ppermute(value, SP, [(i, i + by) for i in range(64 - by)])  23 us
    pallas_call x1, Pallas kernels, local(): call(up_kernel, [smem(), vmem()] + [hbm()] * 11, shape(TOK, FF), [pltpu.V...  9.08 us
    unnamed x42, local copies, waits for them, and re-layouts  7.24 us
    pallas_call x1, Pallas kernels, local(): call(project_kernel, [smem()] + [vmem()] * 4 + [hbm()] * 6, [shape(TOK, D...  5.56 us
    ppermute x4, waiting for transfers between devices, shift_sp(): return lax.ppermute(value, SP, [(i, i + by) for i in range(64 - by)])  5.17 us
  transfers between devices with their start and end apart: 41, of which 19 were waited for; matrix products, arithmetic and copies ran while one was open for 0% of the time, Pallas kernels for 14%

profile of v1, /device:TPU:1, one launch (start us, length us, event | category | flops | bytes accessed | tf_op | source)
XLA Modules:
  0.0 219.8 jit_solution(3738168869466401330)
XLA Ops:
  0.0 2.5 %collective-permute-start.24 = (bf16[32,2048]{1,0:T(8,128)(2,1)}, bf16[32,2048]{1,0:T(8,128)(2,1)S(1)}, u32[]{:S(2)}, u32[]{:S(2)}) collective-permute-start(bf16[32,2048]{1,0:T(8,128)(2,1)} %bitcast.8.own), channel_id=1, source_target_pairs={{0,32},{32,64},{64,96},{96,128},{128,160},{160,192},{192,224},{224... | collective-permute-start | bytes 393224 | tf_op jit(solution)/shard_map/ppermute | solution.py:28
  2.6 4.0 %collective-permute-start.25 = (bf16[32,2048]{1,0:T(8,128)(2,1)}, bf16[32,2048]{1,0:T(8,128)(2,1)S(1)}, u32[]{:S(2)}, u32[]{:S(2)}) collective-permute-start(bf16[32,2048]{1,0:T(8,128)(2,1)} %bitcast.8.own), channel_id=1, source_target_pairs={{0,224},{32,0},{64,32},{96,64},{128,96},{160,128},{192,160},{224,1... | collective-permute-start | bytes 393224 | tf_op jit(solution)/shard_map/ppermute | solution.py:28
  14.5 2.7 %collective-permute-start.12 = (bf16[32,2048]{1,0:T(8,128)(2,1)}, bf16[32,2048]{1,0:T(8,128)(2,1)S(1)}, u32[]{:S(2)}, u32[]{:S(2)}) collective-permute-start(bf16[32,2048]{1,0:T(8,128)(2,1)} %refs_0_.1), channel_id=1, source_target_pairs={{0,24},{8,0},{16,8},{24,16},{1,25},{9,1},{17,9},{25,17},{2,26},{10... | collective-permute-start | bytes 393224 | tf_op jit(solution)/shard_map/ppermute | solution.py:28
  17.6 3.7 %collective-permute-start.26 = (bf16[32,2048]{1,0:T(8,128)(2,1)}, bf16[32,2048]{1,0:T(8,128)(2,1)S(1)}, u32[]{:S(2)}, u32[]{:S(2)}) collective-permute-start(bf16[32,2048]{1,0:T(8,128)(2,1)} %bitcast.8.own), channel_id=1, source_target_pairs={{0,128},{32,160},{64,192},{96,224},{128,0},{160,32},{192,64},{224,... | collective-permute-start | bytes 393224 | tf_op jit(solution)/shard_map/ppermute | solution.py:28
  25.0 5.0 %collective-permute-done.26.p4 = bf16[32,2048]{1,0:T(8,128)(2,1)S(1)} collective-permute-done((bf16[32,2048]{1,0:T(8,128)(2,1)}, bf16[32,2048]{1,0:T(8,128)(2,1)S(1)}, u32[]{:S(2)}, u32[]{:S(2)}) %collective-permute-start.26) | collective-permute-done | bytes 131104 | tf_op jit(solution)/shard_map/ppermute | solution.py:28
  35.3 7.0 %collective-permute-done.14.refs_1_ = bf16[128,2048]{1,0:T(8,128)(2,1)} collective-permute-done((bf16[128,2048]{1,0:T(8,128)(2,1)}, bf16[128,2048]{1,0:T(8,128)(2,1)}, u32[]{:S(2)}, u32[]{:S(2)}) %collective-permute-start.14) | collective-permute-done | bytes 524320 | tf_op jit(solution)/shard_map/ppermute | solution.py:28
  44.9 2.8 %shard_map.136 = (bf16[288,128]{1,0:T(8,128)(2,1)}, f32[512,256]{1,0:T(8,128)S(1)}, f32[512,128]{1,0:T(8,128)S(1)}) custom-call(f32[24,128]{1,0:T(8,128)S(1)} %pad_maximum_fusion.gates_ref, bf16[512,256]{1,0:T(8,128)(2,1)S(1)} %copy-done.2, bf16[512,256]{1,0:T(8,128)(2,1)S(1)} %copy-done.7, bf16[512,256]{1,0:T(8,128)(2,1)S(1)} %copy-done.8), custom_call_target="tpu_custom_call" | custom-call | flops 209715200 | tf_op jit(solution)/shard_map/pallas_call | solution.py:493
  49.1 4.4 %collective-permute-start = (bf16[288,128]{1,0:T(8,128)(2,1)}, bf16[288,128]{1,0:T(8,128)(2,1)S(1)}, u32[]{:S(2)}, u32[]{:S(2)}) collective-permute-start(bf16[288,128]{1,0:T(8,128)(2,1)} %get-tuple-element.25), channel_id=1, source_target_pairs={{0,4},{4,8},{8,12},{12,16},{16,20},{20,24},{24,28},{28,32},{32,36}... | collective-permute-start | bytes 221192 | tf_op jit(solution)/shard_map/ppermute | solution.py:32
  53.5 2.4 %collective-permute-done.s1 = bf16[288,128]{1,0:T(8,128)(2,1)S(1)} collective-permute-done((bf16[288,128]{1,0:T(8,128)(2,1)}, bf16[288,128]{1,0:T(8,128)(2,1)S(1)}, u32[]{:S(2)}, u32[]{:S(2)}) %collective-permute-start) | collective-permute-done | bytes 73760 | tf_op jit(solution)/shard_map/ppermute | solution.py:32
  55.9 3.2 %collective-permute-start.1 = (bf16[288,128]{1,0:T(8,128)(2,1)}, bf16[288,128]{1,0:T(8,128)(2,1)S(1)}, u32[]{:S(2)}, u32[]{:S(2)}) collective-permute-start(bf16[288,128]{1,0:T(8,128)(2,1)} %get-tuple-element.25), channel_id=1, source_target_pairs={{0,8},{4,12},{8,16},{12,20},{16,24},{20,28},{24,32},{28,36},{32,40... | collective-permute-start | bytes 221192 | tf_op jit(solution)/shard_map/ppermute | solution.py:32
  61.4 8.1 %collective-permute-start.2 = (bf16[288,128]{1,0:T(8,128)(2,1)}, bf16[288,128]{1,0:T(8,128)(2,1)}, u32[]{:S(2)}, u32[]{:S(2)}) collective-permute-start(bf16[288,128]{1,0:T(8,128)(2,1)} %get-tuple-element.25), channel_id=1, source_target_pairs={{0,12},{4,16},{8,20},{12,24},{16,28},{20,32},{24,36},{28,40},{32,4... | collective-permute-start | bytes 221192 | tf_op jit(solution)/shard_map/ppermute | solution.py:32
  70.6 7.4 %collective-permute-start.3 = (bf16[288,128]{1,0:T(8,128)(2,1)}, bf16[288,128]{1,0:T(8,128)(2,1)S(1)}, u32[]{:S(2)}, u32[]{:S(2)}) collective-permute-start(bf16[288,128]{1,0:T(8,128)(2,1)} %get-tuple-element.25), channel_id=1, source_target_pairs={{0,16},{4,20},{8,24},{12,28},{16,32},{20,36},{24,40},{28,44},{32,4... | collective-permute-start | bytes 221192 | tf_op jit(solution)/shard_map/ppermute | solution.py:32
  85.7 3.5 %shard_map.137.refs_0_ = bf16[528,256]{1,0:T(8,128)(2,1)S(1)} custom-call(f32[24,128]{1,0:T(8,128)S(1)} %pad_maximum_fusion.gates_ref, bf16[512,256]{1,0:T(8,128)(2,1)S(1)} %copy-done.2, bf16[512,256]{1,0:T(8,128)(2,1)S(1)} %copy-done.9, bf16[1,256]{1,0:T(2,128)(2,1)S(1)} %broadcast_in_dim.3.gain_ref, bf16[4,128]{1,0:T(4,128)(2,1)S(1)} %bitcast.11, ...), custom_call_target="tpu_custom_call" | custom-call | flops 33554432 | tf_op jit(solution)/shard_map/pallas_call | solution.py:532
  89.7 4.4 %collective-permute-done.17.refs_4_ = bf16[128,2048]{1,0:T(8,128)(2,1)S(1)} collective-permute-done((bf16[128,2048]{1,0:T(8,128)(2,1)}, bf16[128,2048]{1,0:T(8,128)(2,1)S(1)}, u32[]{:S(2)}, u32[]{:S(2)}) %collective-permute-start.17) | collective-permute-done | bytes 524320 | tf_op jit(solution)/shard_map/ppermute | solution.py:28
  94.1 5.9 %collective-permute-start.33 = (bf16[768,2048]{1,0:T(8,128)(2,1)S(1)}, bf16[768,2048]{1,0:T(8,128)(2,1)S(1)}, u32[]{:S(2)}, u32[]{:S(2)}) collective-permute-start(bf16[768,2048]{1,0:T(8,128)(2,1)S(1)} %shard_map.148), channel_id=1, source_target_pairs={{0,4},{4,0},{1,5},{5,1},{2,6},{6,2},{3,7},{7,3},{8,12},{12,8},{9,1... | collective-permute-start | bytes 9437192 | tf_op jit(solution)/shard_map/ppermute | solution.py:28
  101.7 33.2 %collective-permute-done.4.refs_1_ = bf16[528,256]{1,0:T(8,128)(2,1)S(1)} collective-permute-done((bf16[528,256]{1,0:T(8,128)(2,1)S(1)}, bf16[528,256]{1,0:T(8,128)(2,1)S(1)}, u32[]{:S(2)}, u32[]{:S(2)}) %collective-permute-start.4) | collective-permute-done | bytes 270368 | tf_op jit(solution)/shard_map/ppermute | solution.py:28
  136.7 2.5 %collective-permute-start.18 = (bf16[128,2048]{1,0:T(8,128)(2,1)}, bf16[128,2048]{1,0:T(8,128)(2,1)S(1)}, u32[]{:S(2)}, u32[]{:S(2)}) collective-permute-start(bf16[128,2048]{1,0:T(8,128)(2,1)} %collective-permute-done.16.refs_3_), channel_id=1, source_target_pairs={{0,32},{32,64},{64,96},{96,128},{128,160},{160,192},{192,224},{224... | collective-permute-start | bytes 1572872 | tf_op jit(solution)/shard_map/ppermute | solution.py:28
  139.3 3.1 %collective-permute-done.5.refs_2_ = bf16[528,256]{1,0:T(8,128)(2,1)S(1)} collective-permute-done((bf16[528,256]{1,0:T(8,128)(2,1)S(1)}, bf16[528,256]{1,0:T(8,128)(2,1)S(1)}, u32[]{:S(2)}, u32[]{:S(2)}) %collective-permute-start.5) | collective-permute-done | bytes 270368 | tf_op jit(solution)/shard_map/ppermute | solution.py:28
  142.4 2.1 collective-permute-start.19
  146.6 3.9 %collective-permute-done.18.refs_0_.refs_5_ = bf16[128,2048]{1,0:T(8,128)(2,1)S(1)} collective-permute-done((bf16[128,2048]{1,0:T(8,128)(2,1)}, bf16[128,2048]{1,0:T(8,128)(2,1)S(1)}, u32[]{:S(2)}, u32[]{:S(2)}) %collective-permute-start.18) | collective-permute-done | bytes 524320 | tf_op jit(solution)/shard_map/ppermute | solution.py:28
  152.3 4.0 %collective-permute-done.19.refs_1_.refs_6_ = bf16[128,2048]{1,0:T(8,128)(2,1)S(1)} collective-permute-done((bf16[128,2048]{1,0:T(8,128)(2,1)S(1)}, bf16[128,2048]{1,0:T(8,128)(2,1)S(1)}, u32[]{:S(2)}, u32[]{:S(2)}) %collective-permute-start.19) | collective-permute-done | bytes 524320 | tf_op jit(solution)/shard_map/ppermute | solution.py:28
  158.0 6.9 %collective-permute-done.31.refs_0_ = bf16[128,2048]{1,0:T(8,128)(2,1)S(1)} collective-permute-done((bf16[128,2048]{1,0:T(8,128)(2,1)S(1)}, bf16[128,2048]{1,0:T(8,128)(2,1)S(1)}, u32[]{:S(2)}, u32[]{:S(2)}) %collective-permute-start.31) | collective-permute-done | bytes 524320 | tf_op jit(solution)/shard_map/ppermute | solution.py:28
  167.9 2.8 %collective-permute-start.22 = (bf16[256,2048]{1,0:T(8,128)(2,1)S(1)}, bf16[256,2048]{1,0:T(8,128)(2,1)S(1)}, u32[]{:S(2)}, u32[]{:S(2)}) collective-permute-start(bf16[256,2048]{1,0:T(8,128)(2,1)S(1)} %shard_map.143), channel_id=1, source_target_pairs={{0,4},{4,0},{1,5},{5,1},{2,6},{6,2},{3,7},{7,3},{8,12},{12,8},{9,1... | collective-permute-start | bytes 3145736 | tf_op jit(solution)/shard_map/ppermute | solution.py:28
  170.7 6.8 %collective-permute-done.20.refs_7_ = bf16[128,2048]{1,0:T(8,128)(2,1)S(1)} collective-permute-done((bf16[128,2048]{1,0:T(8,128)(2,1)S(1)}, bf16[128,2048]{1,0:T(8,128)(2,1)S(1)}, u32[]{:S(2)}, u32[]{:S(2)}) %collective-permute-start.20) | collective-permute-done | bytes 524320 | tf_op jit(solution)/shard_map/ppermute | solution.py:28
  177.6 2.9 %collective-permute-start.34 = (bf16[256,2048]{1,0:T(8,128)(2,1)S(1)}, bf16[256,2048]{1,0:T(8,128)(2,1)S(1)}, u32[]{:S(2)}, u32[]{:S(2)}) collective-permute-start(bf16[256,2048]{1,0:T(8,128)(2,1)S(1)} %shard_map.147.refs_3_), channel_id=1, source_target_pairs={{0,4},{4,0},{1,5},{5,1},{2,6},{6,2},{3,7},{7,3},{8,12},{12,8},{9,1... | collective-permute-start | bytes 3145736 | tf_op jit(solution)/shard_map/ppermute | solution.py:28
  180.4 5.6 %shard_map.140 = (bf16[512,2048]{1,0:T(8,128)(2,1)S(1)}, bf16[512,512]{1,0:T(8,128)(2,1)S(1)}) custom-call(s32[4]{0:T(128)S(1)} %pad_add_fusion.at_ref, bf16[528,256]{1,0:T(8,128)(2,1)S(1)} %shard_map.137.refs_0_, bf16[528,256]{1,0:T(8,128)(2,1)S(1)} %collective-permute-done.4.refs_1_, bf16[528,256]{1,0:T(8,128)(2,1)S(1)} %collective-permute-done.5.refs_2_, ...), custom_call_target="tpu_custom_call" | custom-call | flops 2147483648 | tf_op jit(solution)/shard_map/pallas_call | solution.py:550
  186.0 9.1 %shard_map.144.sq_ref = bf16[512,2048]{1,0:T(8,128)(2,1)S(1)} custom-call(s32[4]{0:T(128)S(1)} %pad_add_fusion.at_ref, bf16[512,2048]{1,0:T(8,128)(2,1)S(1)} %get-tuple-element.27.x_ref, bf16[128,2048]{1,0:T(8,128)(2,1)} %shard_map.141.refs_0_, bf16[128,2048]{1,0:T(8,128)(2,1)} %collective-permute-done.14.refs_1_, ...), custom_call_target="tpu_custom_call" | custom-call | flops 4294967296 | tf_op jit(solution)/shard_map/pallas_call | solution.py:573
  198.4 3.4 %collective-permute-start.39 = (bf16[256,512]{1,0:T(8,128)(2,1)S(1)}, bf16[256,512]{1,0:T(8,128)(2,1)S(1)}, u32[]{:S(2)}, u32[]{:S(2)}) collective-permute-start(bf16[256,512]{1,0:T(8,128)(2,1)S(1)} %get-tuple-element.40), channel_id=1, source_target_pairs={{0,3},{1,0},{2,1},{3,2},{4,7},{5,4},{6,5},{7,6},{8,11},{9,8},{10,9... | collective-permute-start | bytes 786440 | tf_op jit(solution)/shard_map/ppermute | solution.py:28
  201.8 2.6 %shard_map.151 = (bf16[256,512]{1,0:T(8,128)(2,1)S(1)}, bf16[256,512]{1,0:T(8,128)(2,1)S(1)}, bf16[256,512]{1,0:T(8,128)(2,1)S(1)}, bf16[256,512]{1,0:T(8,128)(2,1)S(1)}) custom-call(bf16[512,2048]{1,0:T(8,128)(2,1)S(1)} %shard_map.144.sq_ref, bf16[2,512,2048]{2,1,0:T(8,128)(2,1)S(1)} %get-tuple-element.33.down_ref), custom_call_target="tpu_custom_call" | custom-call | flops 2147483648 | tf_op jit(solution)/shard_map/pallas_call | solution.py:591
  204.5 2.7 %collective-permute-start.38 = (bf16[256,512]{1,0:T(8,128)(2,1)S(1)}, bf16[256,512]{1,0:T(8,128)(2,1)S(1)}, u32[]{:S(2)}, u32[]{:S(2)}) collective-permute-start(bf16[256,512]{1,0:T(8,128)(2,1)S(1)} %get-tuple-element.38), channel_id=1, source_target_pairs={{0,3},{1,0},{2,1},{3,2},{4,7},{5,4},{6,5},{7,6},{8,11},{9,8},{10,9... | collective-permute-start | bytes 786440 | tf_op jit(solution)/shard_map/ppermute | solution.py:28
  208.1 2.7 %collective-permute-start.40 = (bf16[256,512]{1,0:T(8,128)(2,1)S(1)}, bf16[256,512]{1,0:T(8,128)(2,1)S(1)}, u32[]{:S(2)}, u32[]{:S(2)}) collective-permute-start(bf16[256,512]{1,0:T(8,128)(2,1)S(1)} %add_convert_fusion.1), channel_id=1, source_target_pairs={{0,3},{1,0},{2,1},{3,2},{4,7},{5,4},{6,5},{7,6},{8,11},{9,8},{10,9... | collective-permute-start | bytes 786440 | tf_op jit(solution)/shard_map/ppermute | solution.py:28
  213.1 5.6 %collective-permute-done.36 = bf16[256,512]{1,0:T(8,128)(2,1)S(1)} collective-permute-done((bf16[256,512]{1,0:T(8,128)(2,1)S(1)}, bf16[256,512]{1,0:T(8,128)(2,1)S(1)}, u32[]{:S(2)}, u32[]{:S(2)}) %collective-permute-start.36) | collective-permute-done | bytes 262176 | tf_op jit(solution)/shard_map/ppermute | solution.py:28
  (121 shorter events, 52.6 us)
Async XLA Ops:
  0.0 9.9 %collective-permute-start.24 = (bf16[32,2048]{1,0:T(8,128)(2,1)}, bf16[32,2048]{1,0:T(8,128)(2,1)S(1)}, u32[]{:S(2)}, u32[]{:S(2)}) collective-permute-start(bf16[32,2048]{1,0:T(8,128)(2,1)} %bitcast.8.own), channel_id=1, source_target_pairs={{0,32},{32,64},{64,96},{96,128},{128,160},{160,192},{192,224},{224... | collective-permute-start | bytes 393224 | tf_op jit(solution)/shard_map/ppermute | solution.py:28
  6.6 11.0 %collective-permute-start.11 = (bf16[32,2048]{1,0:T(8,128)(2,1)}, bf16[32,2048]{1,0:T(8,128)(2,1)S(1)}, u32[]{:S(2)}, u32[]{:S(2)}) collective-permute-start(bf16[32,2048]{1,0:T(8,128)(2,1)} %refs_0_.1), channel_id=1, source_target_pairs={{0,8},{8,16},{16,24},{24,0},{1,9},{9,17},{17,25},{25,1},{2,10},{10... | collective-permute-start | bytes 393224 | tf_op jit(solution)/shard_map/ppermute | solution.py:28
  10.9 19.2 %collective-permute-start.27 = (bf16[64,2048]{1,0:T(8,128)(2,1)S(1)}, bf16[64,2048]{1,0:T(8,128)(2,1)S(1)}, u32[]{:S(2)}, u32[]{:S(2)}) collective-permute-start(bf16[64,2048]{1,0:T(8,128)(2,1)S(1)} %get-tuple-element.28), channel_id=1, source_target_pairs={{0,64},{32,96},{64,128},{96,160},{128,192},{160,224},{192,0},{224,... | collective-permute-start | bytes 786440 | tf_op jit(solution)/shard_map/ppermute | solution.py:28
  12.6 17.4 %collective-permute-start.28 = (bf16[64,2048]{1,0:T(8,128)(2,1)S(1)}, bf16[64,2048]{1,0:T(8,128)(2,1)S(1)}, u32[]{:S(2)}, u32[]{:S(2)}) collective-permute-start(bf16[64,2048]{1,0:T(8,128)(2,1)S(1)} %get-tuple-element.29), channel_id=1, source_target_pairs={{0,192},{32,224},{64,0},{96,32},{128,64},{160,96},{192,128},{224,1... | collective-permute-start | bytes 786440 | tf_op jit(solution)/shard_map/ppermute | solution.py:28
  17.6 12.4 %collective-permute-start.26 = (bf16[32,2048]{1,0:T(8,128)(2,1)}, bf16[32,2048]{1,0:T(8,128)(2,1)S(1)}, u32[]{:S(2)}, u32[]{:S(2)}) collective-permute-start(bf16[32,2048]{1,0:T(8,128)(2,1)} %bitcast.8.own), channel_id=1, source_target_pairs={{0,128},{32,160},{64,192},{96,224},{128,0},{160,32},{192,64},{224,... | collective-permute-start | bytes 393224 | tf_op jit(solution)/shard_map/ppermute | solution.py:28
  24.8 17.5 %collective-permute-start.14 = (bf16[128,2048]{1,0:T(8,128)(2,1)}, bf16[128,2048]{1,0:T(8,128)(2,1)}, u32[]{:S(2)}, u32[]{:S(2)}) collective-permute-start(bf16[128,2048]{1,0:T(8,128)(2,1)} %shard_map.141.refs_0_), channel_id=1, source_target_pairs={{0,32},{32,64},{64,96},{96,128},{128,160},{160,192},{192,224},{224... | collective-permute-start | bytes 1572872 | tf_op jit(solution)/shard_map/ppermute | solution.py:28
  31.0 54.4 %collective-permute-start.29 = (bf16[256,2048]{1,0:T(8,128)(2,1)S(1)}, bf16[256,2048]{1,0:T(8,128)(2,1)S(1)}, u32[]{:S(2)}, u32[]{:S(2)}) collective-permute-start(bf16[256,2048]{1,0:T(8,128)(2,1)S(1)} %shard_map.146.refs_0_), channel_id=1, source_target_pairs={{0,8},{8,16},{16,24},{24,0},{1,9},{9,17},{17,25},{25,1},{2,10},{10... | collective-permute-start | bytes 3145736 | tf_op jit(solution)/shard_map/ppermute | solution.py:28
  32.4 50.0 %collective-permute-start.15 = (bf16[128,2048]{1,0:T(8,128)(2,1)}, bf16[128,2048]{1,0:T(8,128)(2,1)}, u32[]{:S(2)}, u32[]{:S(2)}) collective-permute-start(bf16[128,2048]{1,0:T(8,128)(2,1)} %shard_map.141.refs_0_), channel_id=1, source_target_pairs={{0,224},{32,0},{64,32},{96,64},{128,96},{160,128},{192,160},{224,1... | collective-permute-start | bytes 1572872 | tf_op jit(solution)/shard_map/ppermute | solution.py:28
  33.8 55.3 %collective-permute-start.30 = (bf16[256,2048]{1,0:T(8,128)(2,1)S(1)}, bf16[256,2048]{1,0:T(8,128)(2,1)S(1)}, u32[]{:S(2)}, u32[]{:S(2)}) collective-permute-start(bf16[256,2048]{1,0:T(8,128)(2,1)S(1)} %shard_map.146.refs_0_), channel_id=1, source_target_pairs={{0,24},{8,0},{16,8},{24,16},{1,25},{9,1},{17,9},{25,17},{2,26},{10... | collective-permute-start | bytes 3145736 | tf_op jit(solution)/shard_map/ppermute | solution.py:28
  42.3 41.6 %collective-permute-start.16 = (bf16[128,2048]{1,0:T(8,128)(2,1)}, bf16[128,2048]{1,0:T(8,128)(2,1)}, u32[]{:S(2)}, u32[]{:S(2)}) collective-permute-start(bf16[128,2048]{1,0:T(8,128)(2,1)} %collective-permute-done.14.refs_1_), channel_id=1, source_target_pairs={{0,32},{32,64},{64,96},{96,128},{128,160},{160,192},{192,224},{224... | collective-permute-start | bytes 1572872 | tf_op jit(solution)/shard_map/ppermute | solution.py:28
  61.4 9.1 %collective-permute-start.2 = (bf16[288,128]{1,0:T(8,128)(2,1)}, bf16[288,128]{1,0:T(8,128)(2,1)}, u32[]{:S(2)}, u32[]{:S(2)}) collective-permute-start(bf16[288,128]{1,0:T(8,128)(2,1)} %get-tuple-element.25), channel_id=1, source_target_pairs={{0,12},{4,16},{8,20},{12,24},{16,28},{20,32},{24,36},{28,40},{32,4... | collective-permute-start | bytes 221192 | tf_op jit(solution)/shard_map/ppermute | solution.py:32
  70.6 10.3 %collective-permute-start.3 = (bf16[288,128]{1,0:T(8,128)(2,1)}, bf16[288,128]{1,0:T(8,128)(2,1)S(1)}, u32[]{:S(2)}, u32[]{:S(2)}) collective-permute-start(bf16[288,128]{1,0:T(8,128)(2,1)} %get-tuple-element.25), channel_id=1, source_target_pairs={{0,16},{4,20},{8,24},{12,28},{16,32},{20,36},{24,40},{28,44},{32,4... | collective-permute-start | bytes 221192 | tf_op jit(solution)/shard_map/ppermute | solution.py:32
  80.9 53.9 %collective-permute-start.7 = (bf16[256,2048]{1,0:T(8,128)(2,1)S(1)}, bf16[256,2048]{1,0:T(8,128)(2,1)S(1)}, u32[]{:S(2)}, u32[]{:S(2)}) collective-permute-start(bf16[256,2048]{1,0:T(8,128)(2,1)S(1)} %shard_map.138), channel_id=1, source_target_pairs={{0,1},{1,2},{2,3},{3,0},{4,5},{5,6},{6,7},{7,4},{8,9},{9,10},{10,1... | collective-permute-start | bytes 3145736 | tf_op jit(solution)/shard_map/ppermute | solution.py:28
  82.4 53.7 %collective-permute-start.8 = (bf16[256,2048]{1,0:T(8,128)(2,1)S(1)}, bf16[256,2048]{1,0:T(8,128)(2,1)S(1)}, u32[]{:S(2)}, u32[]{:S(2)}) collective-permute-start(bf16[256,2048]{1,0:T(8,128)(2,1)S(1)} %shard_map.138), channel_id=1, source_target_pairs={{0,3},{1,0},{2,1},{3,2},{4,7},{5,4},{6,5},{7,6},{8,11},{9,8},{10,9... | collective-permute-start | bytes 3145736 | tf_op jit(solution)/shard_map/ppermute | solution.py:28
  83.9 52.8 %collective-permute-start.9 = (bf16[256,2048]{1,0:T(8,128)(2,1)S(1)}, bf16[256,2048]{1,0:T(8,128)(2,1)S(1)}, u32[]{:S(2)}, u32[]{:S(2)}) collective-permute-start(bf16[256,2048]{1,0:T(8,128)(2,1)S(1)} %shard_map.138), channel_id=1, source_target_pairs={{0,2},{1,3},{2,0},{3,1},{4,6},{5,7},{6,4},{7,5},{8,10},{9,11},{10,... | collective-permute-start | bytes 3145736 | tf_op jit(solution)/shard_map/ppermute | solution.py:28
  85.4 8.7 %collective-permute-start.17 = (bf16[128,2048]{1,0:T(8,128)(2,1)}, bf16[128,2048]{1,0:T(8,128)(2,1)S(1)}, u32[]{:S(2)}, u32[]{:S(2)}) collective-permute-start(bf16[128,2048]{1,0:T(8,128)(2,1)} %collective-permute-done.15.refs_2_), channel_id=1, source_target_pairs={{0,224},{32,0},{64,32},{96,64},{128,96},{160,128},{192,160},{224,1... | collective-permute-start | bytes 1572872 | tf_op jit(solution)/shard_map/ppermute | solution.py:28
  89.1 45.7 %collective-permute-start.4 = (bf16[528,256]{1,0:T(8,128)(2,1)S(1)}, bf16[528,256]{1,0:T(8,128)(2,1)S(1)}, u32[]{:S(2)}, u32[]{:S(2)}) collective-permute-start(bf16[528,256]{1,0:T(8,128)(2,1)S(1)} %shard_map.137.refs_0_), channel_id=1, source_target_pairs={{0,1},{1,2},{2,3},{3,0},{4,5},{5,6},{6,7},{7,4},{8,9},{9,10},{10,1... | collective-permute-start | bytes 811016 | tf_op jit(solution)/shard_map/ppermute | solution.py:28
  94.1 101.0 %collective-permute-start.33 = (bf16[768,2048]{1,0:T(8,128)(2,1)S(1)}, bf16[768,2048]{1,0:T(8,128)(2,1)S(1)}, u32[]{:S(2)}, u32[]{:S(2)}) collective-permute-start(bf16[768,2048]{1,0:T(8,128)(2,1)S(1)} %shard_map.148), channel_id=1, source_target_pairs={{0,4},{4,0},{1,5},{5,1},{2,6},{6,2},{3,7},{7,3},{8,12},{12,8},{9,1... | collective-permute-start | bytes 9437192 | tf_op jit(solution)/shard_map/ppermute | solution.py:28
  134.8 51.2 %collective-permute-start.21 = (bf16[640,2048]{1,0:T(8,128)(2,1)S(1)}, bf16[640,2048]{1,0:T(8,128)(2,1)S(1)}, u32[]{:S(2)}, u32[]{:S(2)}) collective-permute-start(bf16[640,2048]{1,0:T(8,128)(2,1)S(1)} %shard_map.142), channel_id=1, source_target_pairs={{0,4},{4,0},{1,5},{5,1},{2,6},{6,2},{3,7},{7,3},{8,12},{12,8},{9,1... | collective-permute-start | bytes 7864328 | tf_op jit(solution)/shard_map/ppermute | solution.py:28
  136.1 8.8 %collective-permute-start.6 = (bf16[528,256]{1,0:T(8,128)(2,1)S(1)}, bf16[528,256]{1,0:T(8,128)(2,1)S(1)}, u32[]{:S(2)}, u32[]{:S(2)}) collective-permute-start(bf16[528,256]{1,0:T(8,128)(2,1)S(1)} %shard_map.137.refs_0_), channel_id=1, source_target_pairs={{0,2},{1,3},{2,0},{3,1},{4,6},{5,7},{6,4},{7,5},{8,10},{9,11},{10,... | collective-permute-start | bytes 811016 | tf_op jit(solution)/shard_map/ppermute | solution.py:28
  136.7 13.8 %collective-permute-start.18 = (bf16[128,2048]{1,0:T(8,128)(2,1)}, bf16[128,2048]{1,0:T(8,128)(2,1)S(1)}, u32[]{:S(2)}, u32[]{:S(2)}) collective-permute-start(bf16[128,2048]{1,0:T(8,128)(2,1)} %collective-permute-done.16.refs_3_), channel_id=1, source_target_pairs={{0,32},{32,64},{64,96},{96,128},{128,160},{160,192},{192,224},{224... | collective-permute-start | bytes 1572872 | tf_op jit(solution)/shard_map/ppermute | solution.py:28
  142.4 14.0 %collective-permute-start.19 = (bf16[128,2048]{1,0:T(8,128)(2,1)S(1)}, bf16[128,2048]{1,0:T(8,128)(2,1)S(1)}, u32[]{:S(2)}, u32[]{:S(2)}) collective-permute-start(bf16[128,2048]{1,0:T(8,128)(2,1)S(1)} %collective-permute-done.17.refs_4_), channel_id=1, source_target_pairs={{0,224},{32,0},{64,32},{96,64},{128,96},{160,128},{192,160},{224,1... | collective-permute-start | bytes 1572872 | tf_op jit(solution)/shard_map/ppermute | solution.py:28
  144.9 35.5 %collective-permute-start.10 = (bf16[384,2048]{1,0:T(8,128)(2,1)S(1)}, bf16[384,2048]{1,0:T(8,128)(2,1)S(1)}, u32[]{:S(2)}, u32[]{:S(2)}) collective-permute-start(bf16[384,2048]{1,0:T(8,128)(2,1)S(1)} %shard_map.139), channel_id=1, source_target_pairs={{0,4},{4,0},{1,5},{5,1},{2,6},{6,2},{3,7},{7,3},{8,12},{12,8},{9,1... | collective-permute-start | bytes 4718600 | tf_op jit(solution)/shard_map/ppermute | solution.py:28
  150.5 14.3 %collective-permute-start.31 = (bf16[128,2048]{1,0:T(8,128)(2,1)S(1)}, bf16[128,2048]{1,0:T(8,128)(2,1)S(1)}, u32[]{:S(2)}, u32[]{:S(2)}) collective-permute-start(bf16[128,2048]{1,0:T(8,128)(2,1)S(1)} %slice.8), channel_id=1, source_target_pairs={{0,8},{8,16},{16,24},{24,0},{1,9},{9,17},{17,25},{25,1},{2,10},{10... | collective-permute-start | bytes 1572872 | tf_op jit(solution)/shard_map/ppermute | solution.py:28
  156.3 11.6 %collective-permute-start.32 = (bf16[128,2048]{1,0:T(8,128)(2,1)S(1)}, bf16[128,2048]{1,0:T(8,128)(2,1)S(1)}, u32[]{:S(2)}, u32[]{:S(2)}) collective-permute-start(bf16[128,2048]{1,0:T(8,128)(2,1)S(1)} %slice.9), channel_id=1, source_target_pairs={{0,24},{8,0},{16,8},{24,16},{1,25},{9,1},{17,9},{25,17},{2,26},{10... | collective-permute-start | bytes 1572872 | tf_op jit(solution)/shard_map/ppermute | solution.py:28
  164.9 12.7 %collective-permute-start.20 = (bf16[128,2048]{1,0:T(8,128)(2,1)S(1)}, bf16[128,2048]{1,0:T(8,128)(2,1)S(1)}, u32[]{:S(2)}, u32[]{:S(2)}) collective-permute-start(bf16[128,2048]{1,0:T(8,128)(2,1)S(1)} %collective-permute-done.18.refs_0_.refs_5_), channel_id=1, source_target_pairs={{0,32},{32,64},{64,96},{96,128},{128,160},{160,192},{192,224},{224... | collective-permute-start | bytes 1572872 | tf_op jit(solution)/shard_map/ppermute | solution.py:28
  167.9 18.1 %collective-permute-start.22 = (bf16[256,2048]{1,0:T(8,128)(2,1)S(1)}, bf16[256,2048]{1,0:T(8,128)(2,1)S(1)}, u32[]{:S(2)}, u32[]{:S(2)}) collective-permute-start(bf16[256,2048]{1,0:T(8,128)(2,1)S(1)} %shard_map.143), channel_id=1, source_target_pairs={{0,4},{4,0},{1,5},{5,1},{2,6},{6,2},{3,7},{7,3},{8,12},{12,8},{9,1... | collective-permute-start | bytes 3145736 | tf_op jit(solution)/shard_map/ppermute | solution.py:28
  177.6 17.6 %collective-permute-start.34 = (bf16[256,2048]{1,0:T(8,128)(2,1)S(1)}, bf16[256,2048]{1,0:T(8,128)(2,1)S(1)}, u32[]{:S(2)}, u32[]{:S(2)}) collective-permute-start(bf16[256,2048]{1,0:T(8,128)(2,1)S(1)} %shard_map.147.refs_3_), channel_id=1, source_target_pairs={{0,4},{4,0},{1,5},{5,1},{2,6},{6,2},{3,7},{7,3},{8,12},{12,8},{9,1... | collective-permute-start | bytes 3145736 | tf_op jit(solution)/shard_map/ppermute | solution.py:28
  197.7 10.2 %collective-permute-start.35 = (bf16[256,512]{1,0:T(8,128)(2,1)S(1)}, bf16[256,512]{1,0:T(8,128)(2,1)S(1)}, u32[]{:S(2)}, u32[]{:S(2)}) collective-permute-start(bf16[256,512]{1,0:T(8,128)(2,1)S(1)} %get-tuple-element.36), channel_id=1, source_target_pairs={{0,1},{1,2},{2,3},{3,0},{4,5},{5,6},{6,7},{7,4},{8,9},{9,10},{10,1... | collective-permute-start | bytes 786440 | tf_op jit(solution)/shard_map/ppermute | solution.py:28
  198.4 9.7 %collective-permute-start.39 = (bf16[256,512]{1,0:T(8,128)(2,1)S(1)}, bf16[256,512]{1,0:T(8,128)(2,1)S(1)}, u32[]{:S(2)}, u32[]{:S(2)}) collective-permute-start(bf16[256,512]{1,0:T(8,128)(2,1)S(1)} %get-tuple-element.40), channel_id=1, source_target_pairs={{0,3},{1,0},{2,1},{3,2},{4,7},{5,4},{6,5},{7,6},{8,11},{9,8},{10,9... | collective-permute-start | bytes 786440 | tf_op jit(solution)/shard_map/ppermute | solution.py:28
  208.0 10.7 %collective-permute-start.36 = (bf16[256,512]{1,0:T(8,128)(2,1)S(1)}, bf16[256,512]{1,0:T(8,128)(2,1)S(1)}, u32[]{:S(2)}, u32[]{:S(2)}) collective-permute-start(bf16[256,512]{1,0:T(8,128)(2,1)S(1)} %add_convert_fusion.2), channel_id=1, source_target_pairs={{0,1},{1,2},{2,3},{3,0},{4,5},{5,6},{6,7},{7,4},{8,9},{9,10},{10,1... | collective-permute-start | bytes 786440 | tf_op jit(solution)/shard_map/ppermute | solution.py:28
  208.1 10.6 %collective-permute-start.40 = (bf16[256,512]{1,0:T(8,128)(2,1)S(1)}, bf16[256,512]{1,0:T(8,128)(2,1)S(1)}, u32[]{:S(2)}, u32[]{:S(2)}) collective-permute-start(bf16[256,512]{1,0:T(8,128)(2,1)S(1)} %add_convert_fusion.1), channel_id=1, source_target_pairs={{0,3},{1,0},{2,1},{3,2},{4,7},{5,4},{6,5},{7,6},{8,11},{9,8},{10,9... | collective-permute-start | bytes 786440 | tf_op jit(solution)/shard_map/ppermute | solution.py:28
  (30 other events, 434.3 us)
